TPU v7x, 32 devices: a whole 2x2x4 slice. The times are simulated.
32 devices in a mesh: kv: 4 (over y, x), tp: 8 (over z, core).
Axes of the slice: x: 2, y: 2, z: 4, core: 2. Of those that a mesh axis runs over, the one named last changes fastest.
Arguments:
- residual: bfloat16 [128, 4096], P(None, ('kv', 'tp')), may hold values from -20 to 20
- mixer_gain: float32 [4096], P('kv'), may hold values from 0.1 to 1.9
- w_query: bfloat16 [4096, 4096], P('kv', 'tp'), may hold values from -0.09375 to 0.09375
- w_forget: bfloat16 [4096, 4096], P('kv', 'tp'), may hold values from -0.09375 to 0.09375
- w_input: bfloat16 [4096, 4096], P('kv', 'tp'), may hold values from -0.09375 to 0.09375
- w_outgate: bfloat16 [4096, 4096], P('kv', 'tp'), may hold values from -0.09375 to 0.09375
- lower_bound: float32 [4096], P('tp'), may hold values from 0.3 to 0.97
- state: float32 [128, 32, 128, 128], P('kv', 'tp'), may hold values from -6 to 6
- head_gain: float32 [128], replicated, may hold values from 0.1 to 1.9
- w_mix_out: bfloat16 [4096, 4096], P('tp', 'kv'), may hold values from -0.09375 to 0.09375
- ffn_gain: float32 [4096], P('kv'), may hold values from 0.1 to 1.9
- w_gate: bfloat16 [4096, 10752], P('kv', 'tp'), may hold values from -0.09375 to 0.09375
- w_up: bfloat16 [4096, 10752], P('kv', 'tp'), may hold values from -0.09375 to 0.09375
- w_down: bfloat16 [10752, 4096], P('tp', 'kv'), may hold values from -0.0625 to 0.0625
Outputs:
- layer_out: bfloat16 [128, 4096], P(None, ('kv', 'tp'))
- new_state: float32 [128, 32, 128, 128], P('kv', 'tp')
All inputs are finite; a program needn't handle non-finite values.
Results may differ from a plain program's by a relative error of at most 0.015.
Values may be sent and summed in bfloat16 or wider, within the bound.
No kernel may reach another device: no remote copies, remote signals or barrier semaphores. Data moves between devices by JAX's collectives and lax.ppermute only.
A program may use at most 64 MiB of HBM per device.

v0:
```python
import jax
import jax.numpy as jnp
from jax import lax
from jax.sharding import PartitionSpec as P

D = 4096
DK = 128
DV = 128


EPS = 1e-06


def project_row(weight, piece):
    return jnp.dot(piece, weight, preferred_element_type=jnp.float32)


def channel_mix(rows_in, ffn_gain, w_gate, w_up, w_down):
    rows_float = rows_in.astype(jnp.float32)
    squares = jnp.sum(rows_float * rows_float, axis=1)
    scaled = (rows_float * ffn_gain).astype(jnp.bfloat16)
    gate = jnp.dot(scaled, w_gate, preferred_element_type=jnp.float32)
    upper = jnp.dot(scaled, w_up, preferred_element_type=jnp.float32)
    whole_total = lax.psum(squares, "kv")
    gate, upper = (
        lax.psum(gate.astype(jnp.bfloat16), "kv").astype(jnp.float32),
        lax.psum(upper.astype(jnp.bfloat16), "kv").astype(jnp.float32),
    )
    inverse = lax.rsqrt(whole_total / D + EPS)[:, None]
    hidden = (jax.nn.silu(gate * inverse) * (upper * inverse)).astype(jnp.bfloat16)
    terms = jnp.dot(hidden, w_down, preferred_element_type=jnp.float32)
    summed = lax.psum_scatter(
        terms.astype(jnp.bfloat16), "tp", scatter_dimension=1, tiled=True
    ).astype(jnp.float32)
    width = summed.shape[1]
    own = lax.dynamic_slice_in_dim(rows_float, lax.axis_index("tp") * width, width, 1)
    return (own + summed).astype(jnp.bfloat16)


def body(
    residual,
    mixer_gain,
    w_query,
    w_forget,
    w_input,
    w_outgate,
    lower_bound,
    state,
    head_gain,
    w_mix_out,
    ffn_gain,
    w_gate,
    w_up,
    w_down,
):
    local_seqs, local_heads = (state.shape[0], state.shape[1])
    rows = lax.all_gather(residual, "tp", axis=1, tiled=True)
    rows_float = rows.astype(jnp.float32)
    squares = jnp.sum(rows_float * rows_float, axis=1)
    scaled = (rows_float * mixer_gain).astype(jnp.bfloat16)
    part_query = jnp.dot(scaled, w_query, preferred_element_type=jnp.float32)
    part_forget = jnp.dot(scaled, w_forget, preferred_element_type=jnp.float32)
    part_value = jnp.dot(scaled, w_input, preferred_element_type=jnp.float32)
    part_gate = jnp.dot(scaled, w_outgate, preferred_element_type=jnp.float32)
    whole_total = lax.psum(squares, "kv")
    total = lax.dynamic_slice_in_dim(whole_total, lax.axis_index("kv") * local_seqs, local_seqs)
    part_query, part_forget, part_value, part_gate = (
        lax.psum_scatter(part_query, "kv", scatter_dimension=0, tiled=True),
        lax.psum_scatter(part_forget, "kv", scatter_dimension=0, tiled=True),
        lax.psum_scatter(part_value, "kv", scatter_dimension=0, tiled=True),
        lax.psum_scatter(part_gate, "kv", scatter_dimension=0, tiled=True),
    )
    inverse = lax.rsqrt(total / D + EPS)[:, None]
    bound = lower_bound.reshape(local_heads, DK)
    forget_raw = (part_forget * inverse).reshape(local_seqs, local_heads, DK)
    forget = bound + (1.0 - bound) * jax.nn.sigmoid(forget_raw)
    keyvec = (1.0 - bound) * jax.nn.sigmoid(-forget_raw)
    query = jax.nn.silu((part_query * inverse).reshape(local_seqs, local_heads, DK))
    values = (part_value * inverse).reshape(local_seqs, local_heads, DV)
    updated = forget[..., None] * state + keyvec[..., None] * values[:, :, None, :]
    head_out = jnp.einsum("shc,shce->she", query, updated, precision=lax.Precision.HIGHEST)
    inv_head = lax.rsqrt(jnp.mean(head_out * head_out, axis=2, keepdims=True) + EPS)
    out_gate = jax.nn.silu((part_gate * inverse).reshape(local_seqs, local_heads, DV))
    normed = (
        (head_out * inv_head * head_gain * out_gate)
        .reshape(local_seqs, local_heads * DV)
        .astype(jnp.bfloat16)
    )
    terms = project_row(w_mix_out, lax.all_gather(normed, "kv", axis=0, tiled=True))
    mixed = lax.psum(terms, "tp")
    after_mix = (rows_float + mixed).astype(jnp.bfloat16)
    layer_out = channel_mix(after_mix, ffn_gain, w_gate, w_up, w_down)
    return (layer_out, updated)


def solution(mesh):
    in_specs = (
        P(None, ("kv", "tp")),
        P("kv"),
        P("kv", "tp"),
        P("kv", "tp"),
        P("kv", "tp"),
        P("kv", "tp"),
        P("tp"),
        P("kv", "tp", None, None),
        P(),
        P("tp", "kv"),
        P("kv"),
        P("kv", "tp"),
        P("kv", "tp"),
        P("tp", "kv"),
    )
    out_specs = (P(None, ("kv", "tp")), P("kv", "tp", None, None))
    return jax.shard_map(body, mesh=mesh, in_specs=in_specs, out_specs=out_specs, check_vma=False)
```

profile of v0, /device:TPU:0, one launch (start us, length us, event | category | flops | bytes accessed | tf_op | source)
XLA Modules:
  0.0 312.9 jit_solution(12020792351462122957)
XLA Ops:
  7.2 15.1 %all_gather.6 = bf16[128,1024]{1,0:T(8,128)(2,1)S(1)} all-gather(bf16[128,128]{1,0:T(8,128)(2,1)} %param.14), channel_id=1, replica_groups=mesh['kv'=4,'tp'=8] {'tp'}, dimensions={1}, use_global_device_ids=true | all-gather | bytes 294912 | tf_op jit(solution)/shard_map/all_gather | solution.py:57
  22.4 2.3 fusion.10
  24.7 2.2 fusion.8
  27.0 2.3 fusion.6
  29.4 2.3 fusion.12
  31.7 0.1 fusion.1
  31.8 9.9 %psum.35 = f32[128]{0:T(128)S(1)} all-reduce(f32[128]{0:T(128)S(1)} %fusion.1), channel_id=1, replica_groups=mesh['kv'=4,'tp'=8] {'kv'}, use_global_device_ids=true, to_apply=%region_2.0 | all-reduce | flops 128 | bytes 1024 | tf_op jit(solution)/shard_map/psum | solution.py:65
  41.8 0.1 add_rsqrt_fusion.2
  41.8 0.7 broadcast_subtract_fusion
  42.5 6.5 %reduce-scatter.10.cloned.1.call-done = f32[32,512]{1,0:T(8,128)} async-done(((f32[128,512]{1,0:T(8,128)}), f32[32,512]{1,0:T(8,128)}) %reduce-scatter.10.cloned.1.call-update) | async-done | bytes 65552 | tf_op jit(solution)/shard_map/reduce_scatter | solution.py:69
  49.0 27.1 %reduce-scatter.12.cloned.1.call-done = f32[32,512]{1,0:T(8,128)} async-done(((f32[128,512]{1,0:T(8,128)}), f32[32,512]{1,0:T(8,128)}) %reduce-scatter.12.cloned.1.call-update) | async-done | bytes 65552 | tf_op jit(solution)/shard_map/reduce_scatter | solution.py:70
  76.1 27.2 %reduce-scatter.14.cloned.1.call-done = f32[32,512]{1,0:T(8,128)} async-done(((f32[128,512]{1,0:T(8,128)}), f32[32,512]{1,0:T(8,128)}) %reduce-scatter.14.cloned.1.call-update) | async-done | bytes 65552 | tf_op jit(solution)/shard_map/reduce_scatter | solution.py:71
  103.3 27.0 %reduce-scatter.8.cloned.1.call-done = f32[32,512]{1,0:T(8,128)} async-done(((f32[128,512]{1,0:T(8,128)}), f32[32,512]{1,0:T(8,128)}) %reduce-scatter.8.cloned.1.call-update) | async-done | bytes 65552 | tf_op jit(solution)/shard_map/reduce_scatter | solution.py:68
  130.3 1.0 add_divide_fusion.1
  131.6 8.2 %multiply_add_fusion = f32[32,4,128,128]{3,2,1,0:T(8,128)S(1)} fusion(f32[32,4,128,128]{3,2,1,0:T(8,128)} %param.21, f32[32,4,128]{2,1,0:T(4,128)S(1)} %mul.164, f32[32,4,128]{2,1,0:T(4,128)S(1)} %bitcast.35, f32[32,4,128]{2,1,0:T(4,128)S(1)} %bitcast.34), kind=kLoop, calls=%fused_computation | loop fusion | flops 6291456 | bytes 16973824 | tf_op jit(solution)/shard_map/add | solution.py:80
  139.9 3.4 %copy-done.1 = f32[32,4,128,128]{3,2,1,0:T(8,128)} copy-done((f32[32,4,128,128]{3,2,1,0:T(8,128)}, f32[32,4,128,128]{3,2,1,0:T(8,128)S(1)}, u32[]{:S(2)}) %copy-start.1) | copy-done | bytes 8388632
  143.2 7.2 %fusion.18 = f32[32,4,1,128]{3,2,1,0:T(1,128)S(1)} fusion(f32[32,4,128,1]{2,3,1,0:T(1,128)S(1)} %bitcast.33, f32[32,4,128,128]{3,2,1,0:T(8,128)S(1)} %multiply_add_fusion), kind=kOutput, calls=%fused_computation.39 | convolution fusion | flops 25165824 | bytes 8519680 | tf_op jit(solution)/shard_map/shc,shce->she/dot_general | solution.py:81
  150.5 0.1 multiply_reduce_fusion.1
  150.6 0.1 fusion.15
  150.8 8.5 %all_gather.7 = bf16[128,512]{1,0:T(8,128)(2,1)S(1)} all-gather(bf16[32,512]{1,0:T(8,128)(2,1)S(1)} %bitcast.38), channel_id=1, replica_groups=mesh['kv'=4,'tp'=8] {'kv'}, dimensions={0}, use_global_device_ids=true | all-gather | bytes 163840 | tf_op jit(solution)/shard_map/all_gather | solution.py:89
  159.2 1.1 fusion.19
  160.4 56.7 %all-reduce.4.cloned.1.call-done = f32[128,1024]{1,0:T(8,128)} async-done(((f32[128,1024]{1,0:T(8,128)}), f32[128,1024]{1,0:T(8,128)}) %all-reduce.4.cloned.1.call-update) | async-done | bytes 524304 | tf_op jit(solution)/shard_map/psum | solution.py:90
  217.1 1.2 multiply_reduce_fusion
  218.3 1.6 convolution_convert_fusion
  219.9 3.4 %convolution_convert_fusion.1 = bf16[128,1344]{0,1:T(8,128)(2,1)} fusion(bf16[1024,1344]{0,1:T(8,128)(2,1)} %param.25, f32[128,1024]{1,0:T(8,128)S(1)} %get-tuple-element.5, f32[1024]{0:T(1024)S(1)} %copy-done.3), kind=kOutput, calls=%fused_computation.2 | convolution fusion | flops 352755712 | bytes 3624960 | tf_op jit(solution)/shard_map/dot_general | solution.py:22
  223.4 10.2 %psum.38 = f32[128]{0:T(128)S(1)} all-reduce(f32[128]{0:T(128)S(1)} %get-tuple-element.4), channel_id=1, replica_groups=mesh['kv'=4,'tp'=8] {'kv'}, use_global_device_ids=true, to_apply=%region_10.11 | all-reduce | flops 128 | bytes 1024 | tf_op jit(solution)/shard_map/psum | solution.py:24
  233.6 36.4 %all-reduce.6.cloned.1.call-done = (bf16[128,1344]{0,1:T(8,128)(2,1)}, bf16[128,1344]{0,1:T(8,128)(2,1)}) async-done(((bf16[128,1344]{0,1:T(8,128)(2,1)}, bf16[128,1344]{0,1:T(8,128)(2,1)}), (bf16[128,1344]{0,1:T(8,128)(2,1)}, bf16[128,1344]{0,1:T(8,128)(2,1)})) %all-reduce.6.cloned.1.call-update) | async-done | bytes 688144 | tf_op jit(solution)/shard_map/psum | solution.py:27
  270.0 2.8 convolution_convert_fusion.2
  272.7 0.8 copy.18
  273.6 31.0 %reduce-scatter.16.cloned.1.call-done = bf16[128,128]{1,0:T(8,128)(2,1)} async-done(((bf16[1024,128]{1,0:T(8,128)(2,1)}), bf16[128,128]{1,0:T(8,128)(2,1)}) %reduce-scatter.16.cloned.1.call-update) | async-done | bytes 32784
  304.5 0.9 copy.19
  305.4 0.6 add_convert_fusion
  (37 shorter events, 0.7 us)
Async XLA Ops:
  7.2 211.1 %copy-start = (bf16[1024,1344]{0,1:T(8,128)(2,1)S(1)}, bf16[1024,1344]{0,1:T(8,128)(2,1)}, u32[]{:S(2)}) copy-start(bf16[1024,1344]{0,1:T(8,128)(2,1)} %param.26) | copy-start | bytes 8257540
  7.2 124.4 %copy-start.4 = (f32[512]{0:T(512)S(1)}, f32[512]{0:T(512)}, u32[]{:S(2)}) copy-start(f32[512]{0:T(512)} %param.20) | copy-start | bytes 6148
  7.2 41.8 %reduce-scatter.10.cloned.1.call-start = ((), (), s32[]{:S(2)}) async-start(), calls=%async_computation.6 | async-start | bytes 327680 | tf_op jit(solution)/shard_map/reduce_scatter | solution.py:69
  24.7 51.5 %reduce-scatter.12.cloned.1.call-start = ((), (), s32[]{:S(2)}) async-start(), calls=%async_computation.7 | async-start | bytes 327680 | tf_op jit(solution)/shard_map/reduce_scatter | solution.py:70
  27.0 76.3 %reduce-scatter.14.cloned.1.call-start = ((), (), s32[]{:S(2)}) async-start(), calls=%async_computation.8 | async-start | bytes 327680 | tf_op jit(solution)/shard_map/reduce_scatter | solution.py:71
  29.3 101.0 %reduce-scatter.8.cloned.1.call-start = ((), (), s32[]{:S(2)}) async-start(), calls=%async_computation.5 | async-start | bytes 327680 | tf_op jit(solution)/shard_map/reduce_scatter | solution.py:68
  31.7 185.4 %all-reduce.4.cloned.1.call-start = ((), (), s32[]{:S(2)}) async-start(), calls=%async_computation.9 | async-start | bytes 1048576 | tf_op jit(solution)/shard_map/psum | solution.py:90
  139.8 3.4 %copy-start.1 = (f32[32,4,128,128]{3,2,1,0:T(8,128)}, f32[32,4,128,128]{3,2,1,0:T(8,128)S(1)}, u32[]{:S(2)}) copy-start(f32[32,4,128,128]{3,2,1,0:T(8,128)S(1)} %multiply_add_fusion) | copy-start | bytes 25165828
  139.8 10.8 %copy-start.5 = (f32[128]{0:T(128)S(1)}, f32[128]{0:T(128)}, u32[]{:S(2)}) copy-start(f32[128]{0:T(128)} %param.22) | copy-start | bytes 1540
  139.9 19.4 %copy-start.2 = (bf16[512,1024]{1,0:T(8,128)(2,1)S(1)}, bf16[512,1024]{1,0:T(8,128)(2,1)}, u32[]{:S(2)}) copy-start(bf16[512,1024]{1,0:T(8,128)(2,1)} %param.23) | copy-start | bytes 3145732
  139.9 78.4 %copy-start.3 = (f32[1024]{0:T(1024)S(1)}, f32[1024]{0:T(1024)}, u32[]{:S(2)}) copy-start(f32[1024]{0:T(1024)} %param.24) | copy-start | bytes 12292
  160.4 109.6 %all-reduce.6.cloned.1.call-start = ((), (), s32[]{:S(2)}) async-start(), calls=%async_computation.11 | async-start | bytes 1376256 | tf_op jit(solution)/shard_map/psum | solution.py:27
  223.4 81.2 %reduce-scatter.16.cloned.1.call-start = ((), (), s32[]{:S(2)}) async-start(), calls=%async_computation.10 | async-start | bytes 294912
Sparse Core Ops, SparseCore 0:
  24.8 24.1 reduce-scatter.9
  51.7 24.3 reduce-scatter.11
  78.9 24.3 reduce-scatter.13
  105.9 24.3 reduce-scatter.7
  160.5 56.5 all-reduce.3
  223.5 46.4 all-reduce.5
  273.7 30.7 reduce-scatter.15
where the time goes:
time: 314 us; the launch traced here: 313 us
  waiting for transfers between devices  212 us (68%)
  blocking collectives  43.7 us (14%)
  matrix products  25.2 us (8%)
  between operations  14.3 us (5%)
  other arithmetic  12.3 us (4%)
  local copies, waits for them, and re-layouts  5.22 us (2%)
    psum x1, waiting for transfers between devices, body(): mixed = lax.psum(terms, 'tp')  56.7 us
    psum x1, waiting for transfers between devices, channel_mix(): lax.psum(upper.astype(jnp.bfloat16), 'kv').astype(jnp.float32)  36.4 us
    unnamed x8, waiting for transfers between devices  31.1 us
    reduce_scatter x1, waiting for transfers between devices, body(): lax.psum_scatter(part_gate, 'kv', scatter_dimension=0, tiled=True)  27.2 us
    reduce_scatter x1, waiting for transfers between devices, body(): lax.psum_scatter(part_value, 'kv', scatter_dimension=0, tiled=True)  27.1 us
    reduce_scatter x1, waiting for transfers between devices, body(): lax.psum_scatter(part_query, 'kv', scatter_dimension=0, tiled=True)  27 us
    all_gather x1, blocking collectives, body(): rows = lax.all_gather(residual, 'tp', axis=1, tiled=True)  15.1 us
    psum x1, blocking collectives, channel_mix(): whole_total = lax.psum(squares, 'kv')  10.2 us
  transfers between devices with their start and end apart: 7, of which 7 were waited for; matrix products, arithmetic and copies ran while one was open for 2% of the time, Pallas kernels for 0%

commit v1 on v0

v1 whole, which is shorter than its diff:
```python
import functools

import jax
import jax.numpy as jnp
from jax import lax
from jax.experimental import pallas as pl
from jax.experimental.pallas import tpu as pltpu
from jax.sharding import PartitionSpec as P

EPS = 1e-06
LANES = 128
PAIR = 2
BF16 = jnp.bfloat16
F32 = jnp.float32


def exchange(value, axis, size, mask):
    return lax.ppermute(value, axis, [(i, i ^ mask) for i in range(size)])


def call(kernel, out_shape, scratch=(), **kwargs):
    return pl.pallas_call(kernel, out_shape=out_shape, scratch_shapes=list(scratch), **kwargs)


def tail_pieces(total, first_lane):
    lane = lax.broadcasted_iota(jnp.int32, (total.shape[0], LANES), 1) - first_lane
    high = total.astype(BF16).astype(F32)
    middle = (total - high).astype(BF16).astype(F32)
    low = total - high - middle
    zero = jnp.zeros((), F32)
    return jnp.where(
        lane == 0, high, jnp.where(lane == 1, middle, jnp.where(lane == 2, low, zero))
    )


def product(left, right):
    return jnp.dot(left, right, preferred_element_type=F32)


def gather_scaled(near_ref, far_ref, gain_ref, blocks_ref, count):
    own = lax.axis_index("tp")
    squares = None
    for k in range(count):
        for ref, source in ((near_ref, own ^ (PAIR * k)), (far_ref, own ^ (PAIR * k + 1))):
            block = ref[k].astype(F32)
            squares = block * block if squares is None else squares + block * block
            blocks_ref[source] = (block * gain_ref[source]).astype(BF16)
    rows = jnp.concatenate([blocks_ref[j] for j in range(PAIR * count)], axis=1)
    return rows, jnp.sum(squares, axis=1, keepdims=True)


def spread(parts_ref, own_ref, send_refs):
    own = lax.axis_index("kv")
    own_ref[...] = parts_ref[own]
    for mask, ref in enumerate(send_refs, 1):
        ref[...] = parts_ref[own ^ mask].astype(BF16)


def project_kernel(near_ref, far_ref, gain_ref, *refs, count, n_weights, offsets, tail, local):
    weights, outs = refs[:n_weights], refs[n_weights:-2]
    blocks_ref, parts_ref = refs[-2:]
    rows, squares = gather_scaled(near_ref, far_ref, gain_ref, blocks_ref, count)
    groups = parts_ref.shape[0]
    start = tail // LANES * LANES
    pieces = tail_pieces(squares, tail - start)

    def put(value, at):
        for d in range(groups):
            parts_ref[d, :, at : at + value.shape[1]] = value[d * local : (d + 1) * local]

    zero = jnp.zeros((rows.shape[0], LANES), F32)
    put(zero, parts_ref.shape[2] - LANES)
    put(pieces, start)
    for weight, at in zip(weights, offsets):
        put(product(rows, weight[...]), at)
    spread(parts_ref, outs[0], outs[1:])


def project(near, far, gain, weights, offsets, tail, width, n_kv):
    count, seqs, block = near.shape
    local = seqs // n_kv
    kernel = functools.partial(
        project_kernel,
        count=count,
        n_weights=len(weights),
        offsets=offsets,
        tail=tail,
        local=local,
    )
    outs = [jax.ShapeDtypeStruct((local, width), F32)]
    outs += [jax.ShapeDtypeStruct((local, width), BF16)] * (n_kv - 1)
    scratch = [
        pltpu.VMEM((PAIR * count, seqs, block), BF16),
        pltpu.VMEM((n_kv, local, width), F32),
    ]
    gains = gain.reshape(PAIR * count, 1, block)
    return call(kernel, outs, scratch)(near, far, gains, *weights)


def recur_kernel(*refs, n_parts, model, heads, keys, values):
    parts = refs[:n_parts]
    bound_ref, gain_ref, state_ref, new_ref, normed_ref = refs[n_parts:]
    raw = parts[0][...]
    for ref in parts[1:]:
        raw = raw + ref[...].astype(F32)
    total = jnp.sum(raw[:, -LANES:], axis=1, keepdims=True)
    raw = raw * lax.rsqrt(total / model + EPS)
    local = raw.shape[0]
    hid = heads * keys
    bound = bound_ref[...]
    query = jax.nn.silu(raw[:, :hid])
    forget_raw = raw[:, hid : 2 * hid]
    forget = bound + (1.0 - bound) * jax.nn.sigmoid(forget_raw)
    keyvec = (1.0 - bound) * jax.nn.sigmoid(-forget_raw)
    value = raw[:, 2 * hid : 2 * hid + heads * values]
    out_gate = jax.nn.silu(raw[:, 2 * hid + heads * values : 2 * (hid + heads * values)])
    for h in range(heads):
        span = slice(h * keys, (h + 1) * keys)
        columns = jnp.concatenate([query[:, span], forget[:, span], keyvec[:, span]], axis=0).T
        spread_values = slice(h * values, (h + 1) * values)
        rows = []
        for s in range(local):
            q = columns[:, s : s + 1]
            f = columns[:, local + s : local + s + 1]
            k = columns[:, 2 * local + s : 2 * local + s + 1]
            new = f * state_ref[s, h] + k * value[s : s + 1, spread_values]
            new_ref[s, h] = new
            rows.append(jnp.sum(q * new, axis=0, keepdims=True))
        head_out = jnp.concatenate(rows, axis=0)
        scale = lax.rsqrt(jnp.mean(head_out * head_out, axis=1, keepdims=True) + EPS)
        normed = head_out * scale * gain_ref[...] * out_gate[:, spread_values]
        normed_ref[:, spread_values] = normed.astype(BF16)


def recur(parts, lower_bound, head_gain, state, model):
    local, heads, keys, values = state.shape
    step = 8
    width = parts[0].shape[1]
    kernel = functools.partial(
        recur_kernel, n_parts=len(parts), model=model, heads=heads, keys=keys, values=values
    )
    row = lambda i: (i, 0)
    fixed = lambda i: (0, 0)
    cube = pl.BlockSpec((step, heads, keys, values), lambda i: (i, 0, 0, 0))
    return pl.pallas_call(
        kernel,
        grid=(local // step,),
        in_specs=[pl.BlockSpec((step, width), row)] * len(parts)
        + [
            pl.BlockSpec((1, heads * keys), fixed),
            pl.BlockSpec((1, values), fixed),
            cube,
        ],
        out_specs=[cube, pl.BlockSpec((step, heads * values), row)],
        out_shape=[
            jax.ShapeDtypeStruct(state.shape, F32),
            jax.ShapeDtypeStruct((local, heads * values), BF16),
        ],
    )(*parts, lower_bound.reshape(1, heads * keys), head_gain.reshape(1, values), state)


def mix_kernel(*refs, n_parts, local, count):
    parts = refs[:n_parts]
    weight_ref, keep_ref, send_ref, rows_ref, terms_ref = refs[n_parts:]
    own = lax.axis_index("kv")
    core = lax.axis_index("tp") % PAIR
    depth = weight_ref.shape[0]
    for mask, ref in enumerate(parts):
        rows_ref[own ^ mask] = ref[...]
    rows = jnp.concatenate([rows_ref[d] for d in range(n_parts)], axis=0)
    terms = product(rows[:, :depth], weight_ref[...])
    block = terms.shape[1] // (PAIR * count)
    for j in range(PAIR * count):
        terms_ref[j] = terms[:, j * block : (j + 1) * block]
    for z in range(count):
        keep_ref[z] = terms_ref[PAIR * z + core]
        send_ref[z] = terms_ref[PAIR * z + 1 - core].astype(BF16)


def mix(parts, weight, count):
    local, width = parts[0].shape
    n_kv = len(parts)
    seqs = local * n_kv
    block = weight.shape[1] // (PAIR * count)
    kernel = functools.partial(mix_kernel, n_parts=n_kv, local=local, count=count)
    outs = [
        jax.ShapeDtypeStruct((count, seqs, block), F32),
        jax.ShapeDtypeStruct((count, seqs, block), BF16),
    ]
    scratch = [
        pltpu.VMEM((n_kv, local, width), BF16),
        pltpu.VMEM((PAIR * count, seqs, block), F32),
    ]
    return call(kernel, outs, scratch)(*parts, weight)


def fold_kernel(keep_ref, far_ref, own_ref, *send_refs):
    z = lax.axis_index("tp") // PAIR
    own_ref[...] = keep_ref[z] + far_ref[z].astype(F32)
    for mask, ref in enumerate(send_refs, 1):
        ref[...] = (keep_ref[z ^ mask] + far_ref[z ^ mask].astype(F32)).astype(BF16)


def finish_kernel(base_ref, *refs):
    total = base_ref[...].astype(F32)
    for ref in refs[:-1]:
        total = total + ref[...].astype(F32)
    refs[-1][...] = total.astype(BF16)


def reduce_tp(keep, send, base, n_tp):
    count, seqs, block = keep.shape
    far = exchange(send, "tp", n_tp, 1)
    outs = [jax.ShapeDtypeStruct((seqs, block), F32)]
    outs += [jax.ShapeDtypeStruct((seqs, block), BF16)] * (count - 1)
    own, *sends = call(fold_kernel, outs)(keep, far)
    got = [exchange(v, "tp", n_tp, PAIR * k) for k, v in enumerate(sends, 1)]
    return call(finish_kernel, jax.ShapeDtypeStruct((seqs, block), BF16))(base, own, *got)


def gather_tp(block, n_tp):
    count = n_tp // PAIR
    near = jnp.stack([block] + [exchange(block, "tp", n_tp, PAIR * k) for k in range(1, count)])
    return near, exchange(near, "tp", n_tp, 1)


def hidden_kernel(*refs, model, tail):
    raw = refs[0][...]
    for ref in refs[1:-1]:
        raw = raw + ref[...].astype(F32)
    half = raw.shape[1] // 2
    start = tail // LANES * LANES
    lane = lax.broadcasted_iota(jnp.int32, (raw.shape[0], LANES), 1)
    pieces = jnp.where(lane >= tail - start, raw[:, start : start + LANES], 0.0)
    inverse = lax.rsqrt(jnp.sum(pieces, axis=1, keepdims=True) / model + EPS)
    gate = raw[:, :half] * inverse
    refs[-1][...] = (jax.nn.silu(gate) * (raw[:, half:] * inverse)).astype(BF16)


def fast_body(
    residual,
    mixer_gain,
    w_query,
    w_forget,
    w_input,
    w_outgate,
    lower_bound,
    state,
    head_gain,
    w_mix_out,
    ffn_gain,
    w_gate,
    w_up,
    w_down,
    *,
    n_kv,
    n_tp,
):
    count = n_tp // PAIR
    model = residual.shape[1] * n_kv * n_tp
    local = state.shape[0]
    kv_masks = range(1, n_kv)

    near, far = gather_tp(residual, n_tp)
    weights = (w_query, w_forget, w_input, w_outgate)
    offsets, at = [], 0
    for weight in weights:
        offsets.append(at)
        at += weight.shape[1]
    own, *sends = project(near, far, mixer_gain, weights, offsets, at, at + LANES, n_kv)
    parts = [own] + [exchange(v, "kv", n_kv, m) for m, v in zip(kv_masks, sends)]
    new_state, normed = recur(parts, lower_bound, head_gain, state, model)

    parts = [normed] + [exchange(normed, "kv", n_kv, m) for m in kv_masks]
    keep, send = mix(parts, w_mix_out, count)
    after_mix = reduce_tp(keep, send, residual, n_tp)

    near, far = gather_tp(after_mix, n_tp)
    units = w_gate.shape[1]
    padded = (units + 3 + LANES - 1) // LANES * LANES
    own, *sends = project(
        near, far, ffn_gain, (w_gate, w_up), (0, padded), units, 2 * padded, n_kv
    )
    parts = [own] + [exchange(v, "kv", n_kv, m) for m, v in zip(kv_masks, sends)]
    hidden = call(
        functools.partial(hidden_kernel, model=model, tail=units),
        jax.ShapeDtypeStruct((local, padded), BF16),
    )(*parts)
    parts = [hidden] + [exchange(hidden, "kv", n_kv, m) for m in kv_masks]
    keep, send = mix(parts, w_down, count)
    return reduce_tp(keep, send, after_mix, n_tp), new_state


def project_row(weight, piece):
    return jnp.dot(piece, weight, preferred_element_type=jnp.float32)


def channel_mix(rows_in, model, ffn_gain, w_gate, w_up, w_down):
    rows_float = rows_in.astype(jnp.float32)
    squares = jnp.sum(rows_float * rows_float, axis=1)
    scaled = (rows_float * ffn_gain).astype(jnp.bfloat16)
    gate = jnp.dot(scaled, w_gate, preferred_element_type=jnp.float32)
    upper = jnp.dot(scaled, w_up, preferred_element_type=jnp.float32)
    whole_total = lax.psum(squares, "kv")
    gate, upper = (
        lax.psum(gate.astype(jnp.bfloat16), "kv").astype(jnp.float32),
        lax.psum(upper.astype(jnp.bfloat16), "kv").astype(jnp.float32),
    )
    inverse = lax.rsqrt(whole_total / model + EPS)[:, None]
    hidden = (jax.nn.silu(gate * inverse) * (upper * inverse)).astype(jnp.bfloat16)
    terms = jnp.dot(hidden, w_down, preferred_element_type=jnp.float32)
    summed = lax.psum_scatter(
        terms.astype(jnp.bfloat16), "tp", scatter_dimension=1, tiled=True
    ).astype(jnp.float32)
    width = summed.shape[1]
    own = lax.dynamic_slice_in_dim(rows_float, lax.axis_index("tp") * width, width, 1)
    return (own + summed).astype(jnp.bfloat16)


def plain_body(
    residual,
    mixer_gain,
    w_query,
    w_forget,
    w_input,
    w_outgate,
    lower_bound,
    state,
    head_gain,
    w_mix_out,
    ffn_gain,
    w_gate,
    w_up,
    w_down,
    *,
    n_kv,
    n_tp,
):
    local_seqs, local_heads, DK, DV = state.shape
    model = residual.shape[1] * n_kv * n_tp
    rows = lax.all_gather(residual, "tp", axis=1, tiled=True)
    rows_float = rows.astype(jnp.float32)
    squares = jnp.sum(rows_float * rows_float, axis=1)
    scaled = (rows_float * mixer_gain).astype(jnp.bfloat16)
    part_query = jnp.dot(scaled, w_query, preferred_element_type=jnp.float32)
    part_forget = jnp.dot(scaled, w_forget, preferred_element_type=jnp.float32)
    part_value = jnp.dot(scaled, w_input, preferred_element_type=jnp.float32)
    part_gate = jnp.dot(scaled, w_outgate, preferred_element_type=jnp.float32)
    whole_total = lax.psum(squares, "kv")
    total = lax.dynamic_slice_in_dim(whole_total, lax.axis_index("kv") * local_seqs, local_seqs)
    part_query, part_forget, part_value, part_gate = (
        lax.psum_scatter(part_query, "kv", scatter_dimension=0, tiled=True),
        lax.psum_scatter(part_forget, "kv", scatter_dimension=0, tiled=True),
        lax.psum_scatter(part_value, "kv", scatter_dimension=0, tiled=True),
        lax.psum_scatter(part_gate, "kv", scatter_dimension=0, tiled=True),
    )
    inverse = lax.rsqrt(total / model + EPS)[:, None]
    bound = lower_bound.reshape(local_heads, DK)
    forget_raw = (part_forget * inverse).reshape(local_seqs, local_heads, DK)
    forget = bound + (1.0 - bound) * jax.nn.sigmoid(forget_raw)
    keyvec = (1.0 - bound) * jax.nn.sigmoid(-forget_raw)
    query = jax.nn.silu((part_query * inverse).reshape(local_seqs, local_heads, DK))
    values = (part_value * inverse).reshape(local_seqs, local_heads, DV)
    updated = forget[..., None] * state + keyvec[..., None] * values[:, :, None, :]
    head_out = jnp.einsum("shc,shce->she", query, updated, precision=lax.Precision.HIGHEST)
    inv_head = lax.rsqrt(jnp.mean(head_out * head_out, axis=2, keepdims=True) + EPS)
    out_gate = jax.nn.silu((part_gate * inverse).reshape(local_seqs, local_heads, DV))
    normed = (
        (head_out * inv_head * head_gain * out_gate)
        .reshape(local_seqs, local_heads * DV)
        .astype(jnp.bfloat16)
    )
    terms = project_row(w_mix_out, lax.all_gather(normed, "kv", axis=0, tiled=True))
    mixed = lax.psum(terms, "tp")
    after_mix = (rows_float + mixed).astype(jnp.bfloat16)
    layer_out = channel_mix(after_mix, model, ffn_gain, w_gate, w_up, w_down)
    return (layer_out, updated)


def pick_body(*args, n_kv, n_tp):
    residual, state = args[0], args[7]
    powers = n_kv & (n_kv - 1) == 0 and n_tp & (n_tp - 1) == 0 and n_tp > PAIR
    tiled = residual.shape[1] % LANES == 0 and state.shape[0] % 8 == 0
    body = fast_body if powers and tiled else plain_body
    return body(*args, n_kv=n_kv, n_tp=n_tp)


def solution(mesh):
    in_specs = (
        P(None, ("kv", "tp")),
        P("kv"),
        P("kv", "tp"),
        P("kv", "tp"),
        P("kv", "tp"),
        P("kv", "tp"),
        P("tp"),
        P("kv", "tp", None, None),
        P(),
        P("tp", "kv"),
        P("kv"),
        P("kv", "tp"),
        P("kv", "tp"),
        P("tp", "kv"),
    )
    out_specs = (P(None, ("kv", "tp")), P("kv", "tp", None, None))
    body = functools.partial(pick_body, n_kv=mesh.shape["kv"], n_tp=mesh.shape["tp"])
    return jax.shard_map(body, mesh=mesh, in_specs=in_specs, out_specs=out_specs, check_vma=False)
```

time: 314 us -> 128 us (0.41)
  waiting for transfers between devices: 212 us -> 42.4 us
  blocking collectives: 43.7 us -> 0 us
  Pallas kernels: 0 us -> 36.1 us
  starting transfers between devices: 0.29 us -> 33 us
  matrix products: 25.2 us -> 0 us
  between operations: 14.3 us -> 0.74 us
  other arithmetic: 12.3 us -> 1.55 us
  local copies, waits for them, and re-layouts: 5.22 us -> 14.1 us
    psum x2 -> x0, waiting for transfers between devices: 93 us -> none  [the longest x1 56.7 us: body(): mixed = lax.psum(terms, 'tp')]
    reduce_scatter x4 -> x0, waiting for transfers between devices: 87.8 us -> none  [the longest x1 27.2 us: body(): lax.psum_scatter(part_gate, 'kv', scatter_dimension=0, tiled=True)]
    ppermute x0 -> x28, waiting for transfers between devices: none -> 42.4 us  [exchange(): return lax.ppermute(value, axis, [(i, i ^ mask) for i in range(size)])]
    pallas_call x0 -> x10, Pallas kernels: none -> 36.1 us  [the longest x1 13.4 us: recur(): pl.pallas_call(kernel, grid=(local // step,), in_specs=[pl.BlockSpec((ste...]
    ppermute x0 -> x28, starting transfers between devices: none -> 33 us  [exchange(): return lax.ppermute(value, axis, [(i, i ^ mask) for i in range(size)])]
    unnamed x8 -> x0, waiting for transfers between devices: 31.1 us -> none
    dot_general x9 -> x0, matrix products: 25.2 us -> none  [the longest x1 7.25 us: body(): jnp.einsum('shc,shce->she', query, updated, precision=lax.Precision.HIGHEST)]
    all_gather x2 -> x0, blocking collectives: 23.6 us -> none  [the longest x1 15.1 us: body(): rows = lax.all_gather(residual, 'tp', axis=1, tiled=True)]
  transfers between devices with their start and end apart: 7 -> 28, of which waited for: 7 -> 24; matrix products, arithmetic and copies ran while one was open for 2% -> 6% of each run, Pallas kernels for 0% -> 0%
where the time goes in v1:
time: 128 us
  waiting for transfers between devices  42.4 us (33%)
  Pallas kernels  36.1 us (28%)
  starting transfers between devices  33 us (26%)
  local copies, waits for them, and re-layouts  14.1 us (11%)
  other arithmetic  1.55 us (1%)
    ppermute x28, waiting for transfers between devices, exchange(): return lax.ppermute(value, axis, [(i, i ^ mask) for i in range(size)])  42.4 us
    ppermute x28, starting transfers between devices, exchange(): return lax.ppermute(value, axis, [(i, i ^ mask) for i in range(size)])  33 us
    unnamed x52, local copies, waits for them, and re-layouts  14.1 us
    pallas_call x1, Pallas kernels, recur(): pl.pallas_call(kernel, grid=(local // step,), in_specs=[pl.BlockSpec((ste...  13.4 us
    pallas_call x2, Pallas kernels, project(): return call(kernel, outs, scratch)(near, far, gains, *weights)  8.71 us
    pallas_call x2, Pallas kernels, mix(): return call(kernel, outs, scratch)(*parts, weight)  5.89 us
    pallas_call x2, Pallas kernels, reduce_tp(): own, *sends = call(fold_kernel, outs)(keep, far)  3.29 us
    pallas_call x2, Pallas kernels, reduce_tp(): call(finish_kernel, jax.ShapeDtypeStruct((seqs, block), BF16))  2.95 us
  transfers between devices with their start and end apart: 28, of which 24 were waited for; matrix products, arithmetic and copies ran while one was open for 6% of the time, Pallas kernels for 0%

profile of v1, /device:TPU:0, one launch (start us, length us, event | category | flops | bytes accessed | tf_op | source)
XLA Modules:
  0.0 127.9 jit_solution(14059918009960006436)
XLA Ops:
  0.6 4.1 %collective-permute-start.1 = (bf16[128,128]{1,0:T(8,128)(2,1)}, bf16[128,128]{1,0:T(8,128)(2,1)S(1)}, u32[]{:S(2)}, u32[]{:S(2)}) collective-permute-start(bf16[128,128]{1,0:T(8,128)(2,1)} %base_ref.1), channel_id=1, source_target_pairs={{0,4},{1,5},{2,6},{3,7},{4,0},{5,1},{6,2},{7,3},{8,12},{9,13},{10,... | collective-permute-start | bytes 98312 | tf_op jit(solution)/shard_map/ppermute | solution.py:18
  4.8 1.6 %collective-permute-start = (bf16[128,128]{1,0:T(8,128)(2,1)}, bf16[128,128]{1,0:T(8,128)(2,1)S(1)}, u32[]{:S(2)}, u32[]{:S(2)}) collective-permute-start(bf16[128,128]{1,0:T(8,128)(2,1)} %base_ref.1), channel_id=1, source_target_pairs={{0,2},{1,3},{2,0},{3,1},{4,6},{5,7},{6,4},{7,5},{8,10},{9,11},{10,... | collective-permute-start | bytes 98312 | tf_op jit(solution)/shard_map/ppermute | solution.py:18
  7.3 1.6 %collective-permute-done = bf16[128,128]{1,0:T(8,128)(2,1)S(1)} collective-permute-done((bf16[128,128]{1,0:T(8,128)(2,1)}, bf16[128,128]{1,0:T(8,128)(2,1)S(1)}, u32[]{:S(2)}, u32[]{:S(2)}) %collective-permute-start) | collective-permute-done | bytes 32800 | tf_op jit(solution)/shard_map/ppermute | solution.py:18
  8.9 3.4 %collective-permute-done.2 = bf16[128,128]{1,0:T(8,128)(2,1)S(1)} collective-permute-done((bf16[128,128]{1,0:T(8,128)(2,1)}, bf16[128,128]{1,0:T(8,128)(2,1)S(1)}, u32[]{:S(2)}, u32[]{:S(2)}) %collective-permute-start.2) | collective-permute-done | bytes 32800 | tf_op jit(solution)/shard_map/ppermute | solution.py:18
  15.1 3.9 %shard_map.149 = (f32[32,2176]{1,0:T(8,128)}, bf16[32,2176]{1,0:T(8,128)(2,1)}, bf16[32,2176]{1,0:T(8,128)(2,1)}, bf16[32,2176]{1,0:T(8,128)(2,1)}) custom-call(bf16[4,128,128]{2,1,0:T(8,128)(2,1)} %copy-done.2, bf16[4,128,128]{2,1,0:T(8,128)(2,1)} %copy-done.12, f32[8,1,128]{2,1,0:T(1,128)} %bitcast.20, bf16[1024,512]{1,0:T(8,128)(2,1)} %refs_0_.2, ...), custom_call_target="tpu_custom_call" | custom-call | tf_op jit(solution)/shard_map/pallas_call | solution.py:97
  20.5 1.5 %collective-permute-start.5 = (bf16[32,2176]{1,0:T(8,128)(2,1)}, bf16[32,2176]{1,0:T(8,128)(2,1)S(1)}, u32[]{:S(2)}, u32[]{:S(2)}) collective-permute-start(bf16[32,2176]{1,0:T(8,128)(2,1)} %get-tuple-element.26), channel_id=1, source_target_pairs={{0,16},{8,24},{16,0},{24,8},{1,17},{9,25},{17,1},{25,9},{2,18},{10... | collective-permute-start | bytes 417800 | tf_op jit(solution)/shard_map/ppermute | solution.py:18
  22.5 3.0 %collective-permute-done.4.refs_1_ = bf16[32,2176]{1,0:T(8,128)(2,1)S(1)} collective-permute-done((bf16[32,2176]{1,0:T(8,128)(2,1)}, bf16[32,2176]{1,0:T(8,128)(2,1)S(1)}, u32[]{:S(2)}, u32[]{:S(2)}) %collective-permute-start.4) | collective-permute-done | bytes 139296 | tf_op jit(solution)/shard_map/ppermute | solution.py:18
  25.6 3.6 %collective-permute-done.5.refs_2_ = bf16[32,2176]{1,0:T(8,128)(2,1)S(1)} collective-permute-done((bf16[32,2176]{1,0:T(8,128)(2,1)}, bf16[32,2176]{1,0:T(8,128)(2,1)S(1)}, u32[]{:S(2)}, u32[]{:S(2)}) %collective-permute-start.5) | collective-permute-done | bytes 139296 | tf_op jit(solution)/shard_map/ppermute | solution.py:18
  29.9 13.4 %shard_map.150 = (f32[32,4,128,128]{3,2,1,0:T(8,128)}, bf16[32,512]{1,0:T(8,128)(2,1)}) custom-call(f32[32,2176]{1,0:T(8,128)} %get-tuple-element.24.refs_0_, bf16[32,2176]{1,0:T(8,128)(2,1)} %copy-done.6, bf16[32,2176]{1,0:T(8,128)(2,1)} %copy-done.7, bf16[32,2176]{1,0:T(8,128)(2,1)} %copy-done.8, f32[1,512]{1,0:T(1,128)} %bitcast.22, f32[1,128]{1,0:T(1,128)} %bitcast.23, ...), custom_call_target="tpu_custom_call" | custom-call | tf_op jit(solution)/shard_map/pallas_call | solution.py:145
  43.2 1.5 %collective-permute-start.9 = (bf16[32,512]{1,0:T(8,128)(2,1)}, bf16[32,512]{1,0:T(8,128)(2,1)S(1)}, u32[]{:S(2)}, u32[]{:S(2)}) collective-permute-start(bf16[32,512]{1,0:T(8,128)(2,1)} %get-tuple-element.28.refs_0_), channel_id=1, source_target_pairs={{0,24},{8,16},{16,8},{24,0},{1,25},{9,17},{17,9},{25,1},{2,26},{10... | collective-permute-start | bytes 98312 | tf_op jit(solution)/shard_map/ppermute | solution.py:18
  46.7 1.5 %collective-permute-done.9.refs_3_ = bf16[32,512]{1,0:T(8,128)(2,1)S(1)} collective-permute-done((bf16[32,512]{1,0:T(8,128)(2,1)}, bf16[32,512]{1,0:T(8,128)(2,1)S(1)}, u32[]{:S(2)}, u32[]{:S(2)}) %collective-permute-start.9) | collective-permute-done | bytes 32800 | tf_op jit(solution)/shard_map/ppermute | solution.py:18
  50.6 2.5 %shard_map.151 = (f32[4,128,128]{2,1,0:T(8,128)}, bf16[4,128,128]{2,1,0:T(8,128)(2,1)}) custom-call(bf16[32,512]{1,0:T(8,128)(2,1)} %get-tuple-element.28.refs_0_, bf16[32,512]{1,0:T(8,128)(2,1)} %copy-done.24, bf16[32,512]{1,0:T(8,128)(2,1)} %copy-done.21, bf16[32,512]{1,0:T(8,128)(2,1)} %copy-done.18, bf16[512,1024]{1,0:T(8,128)(2,1)} %refs_4_.2), custom_call_target="tpu_custom_call" | custom-call | tf_op jit(solution)/shard_map/pallas_call | solution.py:194
  53.1 1.6 %collective-permute-done.10.far_ref = bf16[4,128,128]{2,1,0:T(8,128)(2,1)S(1)} collective-permute-done((bf16[4,128,128]{2,1,0:T(8,128)(2,1)}, bf16[4,128,128]{2,1,0:T(8,128)(2,1)S(1)}, u32[]{:S(2)}, u32[]{:S(2)}) %collective-permute-start.10) | collective-permute-done | bytes 131104 | tf_op jit(solution)/shard_map/ppermute | solution.py:18
  55.3 1.6 %shard_map.152 = (f32[128,128]{1,0:T(8,128)}, bf16[128,128]{1,0:T(8,128)(2,1)}, bf16[128,128]{1,0:T(8,128)(2,1)}, bf16[128,128]{1,0:T(8,128)(2,1)}) custom-call(f32[4,128,128]{2,1,0:T(8,128)} %get-tuple-element.29.keep_ref, bf16[4,128,128]{2,1,0:T(8,128)(2,1)} %copy-done.9), custom_call_target="tpu_custom_call" | custom-call | tf_op jit(solution)/shard_map/pallas_call | solution.py:216
  57.8 3.5 %collective-permute-start.13 = (bf16[128,128]{1,0:T(8,128)(2,1)}, bf16[128,128]{1,0:T(8,128)(2,1)S(1)}, u32[]{:S(2)}, u32[]{:S(2)}) collective-permute-start(bf16[128,128]{1,0:T(8,128)(2,1)} %get-tuple-element.34), channel_id=1, source_target_pairs={{0,6},{1,7},{2,4},{3,5},{4,2},{5,3},{6,0},{7,1},{8,14},{9,15},{10,... | collective-permute-start | bytes 98312 | tf_op jit(solution)/shard_map/ppermute | solution.py:18
  61.9 1.8 %collective-permute-done.13.refs_3_ = bf16[128,128]{1,0:T(8,128)(2,1)S(1)} collective-permute-done((bf16[128,128]{1,0:T(8,128)(2,1)}, bf16[128,128]{1,0:T(8,128)(2,1)S(1)}, u32[]{:S(2)}, u32[]{:S(2)}) %collective-permute-start.13) | collective-permute-done | bytes 32800 | tf_op jit(solution)/shard_map/ppermute | solution.py:18
  65.8 3.5 %collective-permute-start.16 = (bf16[128,128]{1,0:T(8,128)(2,1)}, bf16[128,128]{1,0:T(8,128)(2,1)S(1)}, u32[]{:S(2)}, u32[]{:S(2)}) collective-permute-start(bf16[128,128]{1,0:T(8,128)(2,1)} %shard_map.153.base_ref), channel_id=1, source_target_pairs={{0,6},{1,7},{2,4},{3,5},{4,2},{5,3},{6,0},{7,1},{8,14},{9,15},{10,... | collective-permute-start | bytes 98312 | tf_op jit(solution)/shard_map/ppermute | solution.py:18
  70.2 1.6 %collective-permute-done.16 = bf16[128,128]{1,0:T(8,128)(2,1)S(1)} collective-permute-done((bf16[128,128]{1,0:T(8,128)(2,1)}, bf16[128,128]{1,0:T(8,128)(2,1)S(1)}, u32[]{:S(2)}, u32[]{:S(2)}) %collective-permute-start.16) | collective-permute-done | bytes 32800 | tf_op jit(solution)/shard_map/ppermute | solution.py:18
  71.8 2.5 %collective-permute-done.15 = bf16[128,128]{1,0:T(8,128)(2,1)S(1)} collective-permute-done((bf16[128,128]{1,0:T(8,128)(2,1)}, bf16[128,128]{1,0:T(8,128)(2,1)S(1)}, u32[]{:S(2)}, u32[]{:S(2)}) %collective-permute-start.15) | collective-permute-done | bytes 32800 | tf_op jit(solution)/shard_map/ppermute | solution.py:18
  75.2 2.9 %copy.16.refs_0_ = bf16[1024,1344]{1,0:T(8,128)(2,1)} copy(bf16[1024,1344]{0,1:T(8,128)(2,1)S(1)} %copy-done) | data formatting | bytes 5505024 | tf_op args[11]
  78.1 4.5 %copy.17.refs_1_ = bf16[1024,1344]{1,0:T(8,128)(2,1)} copy(bf16[1024,1344]{0,1:T(8,128)(2,1)} %param.26) | data formatting | bytes 5505024 | tf_op args[12]
  83.3 4.8 %shard_map.154 = (f32[32,2816]{1,0:T(8,128)}, bf16[32,2816]{1,0:T(8,128)(2,1)}, bf16[32,2816]{1,0:T(8,128)(2,1)}, bf16[32,2816]{1,0:T(8,128)(2,1)}) custom-call(bf16[4,128,128]{2,1,0:T(8,128)(2,1)} %copy-done.1, bf16[4,128,128]{2,1,0:T(8,128)(2,1)} %copy-done.10, f32[8,1,128]{2,1,0:T(1,128)} %bitcast.21, bf16[1024,1344]{1,0:T(8,128)(2,1)} %copy.16.refs_0_, ...), custom_call_target="tpu_custom_call" | custom-call | tf_op jit(solution)/shard_map/pallas_call | solution.py:97
  91.5 4.1 %collective-permute-done.18.refs_1_ = bf16[32,2816]{1,0:T(8,128)(2,1)S(1)} collective-permute-done((bf16[32,2816]{1,0:T(8,128)(2,1)}, bf16[32,2816]{1,0:T(8,128)(2,1)S(1)}, u32[]{:S(2)}, u32[]{:S(2)}) %collective-permute-start.18) | collective-permute-done | bytes 180256 | tf_op jit(solution)/shard_map/ppermute | solution.py:18
  95.7 4.0 %collective-permute-done.19.refs_2_ = bf16[32,2816]{1,0:T(8,128)(2,1)S(1)} collective-permute-done((bf16[32,2816]{1,0:T(8,128)(2,1)}, bf16[32,2816]{1,0:T(8,128)(2,1)S(1)}, u32[]{:S(2)}, u32[]{:S(2)}) %collective-permute-start.19) | collective-permute-done | bytes 180256 | tf_op jit(solution)/shard_map/ppermute | solution.py:18
  100.5 1.9 %shard_map.155.refs_0_ = bf16[32,1408]{1,0:T(8,128)(2,1)} custom-call(f32[32,2816]{1,0:T(8,128)} %get-tuple-element.35.refs_0_, bf16[32,2816]{1,0:T(8,128)(2,1)} %copy-done.3, bf16[32,2816]{1,0:T(8,128)(2,1)} %copy-done.4, bf16[32,2816]{1,0:T(8,128)(2,1)} %copy-done.5), custom_call_target="tpu_custom_call" | custom-call | tf_op jit(solution)/shard_map/pallas_call | solution.py:285
  105.9 3.0 %collective-permute-done.23.refs_3_ = bf16[32,1408]{1,0:T(8,128)(2,1)S(1)} collective-permute-done((bf16[32,1408]{1,0:T(8,128)(2,1)}, bf16[32,1408]{1,0:T(8,128)(2,1)S(1)}, u32[]{:S(2)}, u32[]{:S(2)}) %collective-permute-start.23) | collective-permute-done | bytes 90144 | tf_op jit(solution)/shard_map/ppermute | solution.py:18
  110.6 3.4 %shard_map.156 = (f32[4,128,128]{2,1,0:T(8,128)}, bf16[4,128,128]{2,1,0:T(8,128)(2,1)}) custom-call(bf16[32,1408]{1,0:T(8,128)(2,1)} %shard_map.155.refs_0_, bf16[32,1408]{1,0:T(8,128)(2,1)} %copy-done.15, bf16[32,1408]{1,0:T(8,128)(2,1)} %copy-done.14, bf16[32,1408]{1,0:T(8,128)(2,1)} %copy-done.13, bf16[1344,1024]{1,0:T(8,128)(2,1)} %refs_4_.3), custom_call_target="tpu_custom_call" | custom-call | tf_op jit(solution)/shard_map/pallas_call | solution.py:194
  114.0 1.6 %collective-permute-done.24.far_ref = bf16[4,128,128]{2,1,0:T(8,128)(2,1)S(1)} collective-permute-done((bf16[4,128,128]{2,1,0:T(8,128)(2,1)}, bf16[4,128,128]{2,1,0:T(8,128)(2,1)S(1)}, u32[]{:S(2)}, u32[]{:S(2)}) %collective-permute-start.24) | collective-permute-done | bytes 131104 | tf_op jit(solution)/shard_map/ppermute | solution.py:18
  116.2 1.6 %shard_map.157 = (f32[128,128]{1,0:T(8,128)}, bf16[128,128]{1,0:T(8,128)(2,1)}, bf16[128,128]{1,0:T(8,128)(2,1)}, bf16[128,128]{1,0:T(8,128)(2,1)}) custom-call(f32[4,128,128]{2,1,0:T(8,128)} %get-tuple-element.39.keep_ref, bf16[4,128,128]{2,1,0:T(8,128)(2,1)} %copy-done.11), custom_call_target="tpu_custom_call" | custom-call | tf_op jit(solution)/shard_map/pallas_call | solution.py:216
  117.8 2.0 %collective-permute-start.26 = (bf16[128,128]{1,0:T(8,128)(2,1)}, bf16[128,128]{1,0:T(8,128)(2,1)S(1)}, u32[]{:S(2)}, u32[]{:S(2)}) collective-permute-start(bf16[128,128]{1,0:T(8,128)(2,1)} %get-tuple-element.43), channel_id=1, source_target_pairs={{0,4},{1,5},{2,6},{3,7},{4,0},{5,1},{6,2},{7,3},{8,12},{9,13},{10,... | collective-permute-start | bytes 98312 | tf_op jit(solution)/shard_map/ppermute | solution.py:18
  119.9 2.3 %collective-permute-start.27 = (bf16[128,128]{1,0:T(8,128)(2,1)}, bf16[128,128]{1,0:T(8,128)(2,1)S(1)}, u32[]{:S(2)}, u32[]{:S(2)}) collective-permute-start(bf16[128,128]{1,0:T(8,128)(2,1)} %get-tuple-element.44), channel_id=1, source_target_pairs={{0,6},{1,7},{2,4},{3,5},{4,2},{5,3},{6,0},{7,1},{8,14},{9,15},{10,... | collective-permute-start | bytes 98312 | tf_op jit(solution)/shard_map/ppermute | solution.py:18
  122.9 2.9 %collective-permute-done.27.refs_3_ = bf16[128,128]{1,0:T(8,128)(2,1)S(1)} collective-permute-done((bf16[128,128]{1,0:T(8,128)(2,1)}, bf16[128,128]{1,0:T(8,128)(2,1)S(1)}, u32[]{:S(2)}, u32[]{:S(2)}) %collective-permute-start.27) | collective-permute-done | bytes 32800 | tf_op jit(solution)/shard_map/ppermute | solution.py:18
  (88 shorter events, 30.2 us)
Async XLA Ops:
  0.6 6.7 %collective-permute-start.1 = (bf16[128,128]{1,0:T(8,128)(2,1)}, bf16[128,128]{1,0:T(8,128)(2,1)S(1)}, u32[]{:S(2)}, u32[]{:S(2)}) collective-permute-start(bf16[128,128]{1,0:T(8,128)(2,1)} %base_ref.1), channel_id=1, source_target_pairs={{0,4},{1,5},{2,6},{3,7},{4,0},{5,1},{6,2},{7,3},{8,12},{9,13},{10,... | collective-permute-start | bytes 98312 | tf_op jit(solution)/shard_map/ppermute | solution.py:18
  4.8 4.1 %collective-permute-start = (bf16[128,128]{1,0:T(8,128)(2,1)}, bf16[128,128]{1,0:T(8,128)(2,1)S(1)}, u32[]{:S(2)}, u32[]{:S(2)}) collective-permute-start(bf16[128,128]{1,0:T(8,128)(2,1)} %base_ref.1), channel_id=1, source_target_pairs={{0,2},{1,3},{2,0},{3,1},{4,6},{5,7},{6,4},{7,5},{8,10},{9,11},{10,... | collective-permute-start | bytes 98312 | tf_op jit(solution)/shard_map/ppermute | solution.py:18
  6.3 5.9 %collective-permute-start.2 = (bf16[128,128]{1,0:T(8,128)(2,1)}, bf16[128,128]{1,0:T(8,128)(2,1)S(1)}, u32[]{:S(2)}, u32[]{:S(2)}) collective-permute-start(bf16[128,128]{1,0:T(8,128)(2,1)} %base_ref.1), channel_id=1, source_target_pairs={{0,6},{1,7},{2,4},{3,5},{4,2},{5,3},{6,0},{7,1},{8,14},{9,15},{10,... | collective-permute-start | bytes 98312 | tf_op jit(solution)/shard_map/ppermute | solution.py:18
  13.0 1.4 %collective-permute-start.3 = (bf16[4,128,128]{2,1,0:T(8,128)(2,1)S(1)}, bf16[4,128,128]{2,1,0:T(8,128)(2,1)S(1)}, u32[]{:S(2)}, u32[]{:S(2)}) collective-permute-start(bf16[4,128,128]{2,1,0:T(8,128)(2,1)S(1)} %pad_maximum_fusion.near_ref), channel_id=1, source_target_pairs={{0,1},{1,0},{2,3},{3,2},{4,5},{5,4},{6,7},{7,6},{8,9},{9,8},{10,11... | collective-permute-start | bytes 393224 | tf_op jit(solution)/shard_map/ppermute | solution.py:18
  19.0 6.5 %collective-permute-start.4 = (bf16[32,2176]{1,0:T(8,128)(2,1)}, bf16[32,2176]{1,0:T(8,128)(2,1)S(1)}, u32[]{:S(2)}, u32[]{:S(2)}) collective-permute-start(bf16[32,2176]{1,0:T(8,128)(2,1)} %get-tuple-element.25), channel_id=1, source_target_pairs={{0,8},{8,0},{16,24},{24,16},{1,9},{9,1},{17,25},{25,17},{2,10},{10... | collective-permute-start | bytes 417800 | tf_op jit(solution)/shard_map/ppermute | solution.py:18
  20.5 8.6 %collective-permute-start.5 = (bf16[32,2176]{1,0:T(8,128)(2,1)}, bf16[32,2176]{1,0:T(8,128)(2,1)S(1)}, u32[]{:S(2)}, u32[]{:S(2)}) collective-permute-start(bf16[32,2176]{1,0:T(8,128)(2,1)} %get-tuple-element.26), channel_id=1, source_target_pairs={{0,16},{8,24},{16,0},{24,8},{1,17},{9,25},{17,1},{25,9},{2,18},{10... | collective-permute-start | bytes 417800 | tf_op jit(solution)/shard_map/ppermute | solution.py:18
  22.0 7.1 %collective-permute-start.6 = (bf16[32,2176]{1,0:T(8,128)(2,1)}, bf16[32,2176]{1,0:T(8,128)(2,1)S(1)}, u32[]{:S(2)}, u32[]{:S(2)}) collective-permute-start(bf16[32,2176]{1,0:T(8,128)(2,1)} %get-tuple-element.27), channel_id=1, source_target_pairs={{0,24},{8,16},{16,8},{24,0},{1,25},{9,17},{17,9},{25,1},{2,26},{10... | collective-permute-start | bytes 417800 | tf_op jit(solution)/shard_map/ppermute | solution.py:18
  25.6 3.6 %copy-start.6 = (bf16[32,2176]{1,0:T(8,128)(2,1)}, bf16[32,2176]{1,0:T(8,128)(2,1)S(1)}, u32[]{:S(2)}) copy-start(bf16[32,2176]{1,0:T(8,128)(2,1)S(1)} %collective-permute-done.4.refs_1_) | copy-start | bytes 417796
  29.9 45.3 %copy-start = (bf16[1024,1344]{0,1:T(8,128)(2,1)S(1)}, bf16[1024,1344]{0,1:T(8,128)(2,1)}, u32[]{:S(2)}) copy-start(bf16[1024,1344]{0,1:T(8,128)(2,1)} %param.25) | copy-start | bytes 8257540
  43.2 5.0 %collective-permute-start.9 = (bf16[32,512]{1,0:T(8,128)(2,1)}, bf16[32,512]{1,0:T(8,128)(2,1)S(1)}, u32[]{:S(2)}, u32[]{:S(2)}) collective-permute-start(bf16[32,512]{1,0:T(8,128)(2,1)} %get-tuple-element.28.refs_0_), channel_id=1, source_target_pairs={{0,24},{8,16},{16,8},{24,0},{1,25},{9,17},{17,9},{25,1},{2,26},{10... | collective-permute-start | bytes 98312 | tf_op jit(solution)/shard_map/ppermute | solution.py:18
  44.7 4.1 %collective-permute-start.8 = (bf16[32,512]{1,0:T(8,128)(2,1)}, bf16[32,512]{1,0:T(8,128)(2,1)S(1)}, u32[]{:S(2)}, u32[]{:S(2)}) collective-permute-start(bf16[32,512]{1,0:T(8,128)(2,1)} %get-tuple-element.28.refs_0_), channel_id=1, source_target_pairs={{0,16},{8,24},{16,0},{24,8},{1,17},{9,25},{17,1},{25,9},{2,18},{10... | collective-permute-start | bytes 98312 | tf_op jit(solution)/shard_map/ppermute | solution.py:18
  45.9 4.1 %collective-permute-start.7 = (bf16[32,512]{1,0:T(8,128)(2,1)}, bf16[32,512]{1,0:T(8,128)(2,1)S(1)}, u32[]{:S(2)}, u32[]{:S(2)}) collective-permute-start(bf16[32,512]{1,0:T(8,128)(2,1)} %get-tuple-element.28.refs_0_), channel_id=1, source_target_pairs={{0,8},{8,0},{16,24},{24,16},{1,9},{9,1},{17,25},{25,17},{2,10},{10... | collective-permute-start | bytes 98312 | tf_op jit(solution)/shard_map/ppermute | solution.py:18
  53.1 1.6 %collective-permute-start.10 = (bf16[4,128,128]{2,1,0:T(8,128)(2,1)}, bf16[4,128,128]{2,1,0:T(8,128)(2,1)S(1)}, u32[]{:S(2)}, u32[]{:S(2)}) collective-permute-start(bf16[4,128,128]{2,1,0:T(8,128)(2,1)} %get-tuple-element.30), channel_id=1, source_target_pairs={{0,1},{1,0},{2,3},{3,2},{4,5},{5,4},{6,7},{7,6},{8,9},{9,8},{10,11... | collective-permute-start | bytes 393224 | tf_op jit(solution)/shard_map/ppermute | solution.py:18
  56.9 4.5 %collective-permute-start.11 = (bf16[128,128]{1,0:T(8,128)(2,1)}, bf16[128,128]{1,0:T(8,128)(2,1)S(1)}, u32[]{:S(2)}, u32[]{:S(2)}) collective-permute-start(bf16[128,128]{1,0:T(8,128)(2,1)} %get-tuple-element.32), channel_id=1, source_target_pairs={{0,2},{1,3},{2,0},{3,1},{4,6},{5,7},{6,4},{7,5},{8,10},{9,11},{10,... | collective-permute-start | bytes 98312 | tf_op jit(solution)/shard_map/ppermute | solution.py:18
  56.9 5.0 %collective-permute-start.12 = (bf16[128,128]{1,0:T(8,128)(2,1)}, bf16[128,128]{1,0:T(8,128)(2,1)S(1)}, u32[]{:S(2)}, u32[]{:S(2)}) collective-permute-start(bf16[128,128]{1,0:T(8,128)(2,1)} %get-tuple-element.33), channel_id=1, source_target_pairs={{0,4},{1,5},{2,6},{3,7},{4,0},{5,1},{6,2},{7,3},{8,12},{9,13},{10,... | collective-permute-start | bytes 98312 | tf_op jit(solution)/shard_map/ppermute | solution.py:18
  57.8 5.9 %collective-permute-start.13 = (bf16[128,128]{1,0:T(8,128)(2,1)}, bf16[128,128]{1,0:T(8,128)(2,1)S(1)}, u32[]{:S(2)}, u32[]{:S(2)}) collective-permute-start(bf16[128,128]{1,0:T(8,128)(2,1)} %get-tuple-element.34), channel_id=1, source_target_pairs={{0,6},{1,7},{2,4},{3,5},{4,2},{5,3},{6,0},{7,1},{8,14},{9,15},{10,... | collective-permute-start | bytes 98312 | tf_op jit(solution)/shard_map/ppermute | solution.py:18
  65.8 6.0 %collective-permute-start.16 = (bf16[128,128]{1,0:T(8,128)(2,1)}, bf16[128,128]{1,0:T(8,128)(2,1)S(1)}, u32[]{:S(2)}, u32[]{:S(2)}) collective-permute-start(bf16[128,128]{1,0:T(8,128)(2,1)} %shard_map.153.base_ref), channel_id=1, source_target_pairs={{0,6},{1,7},{2,4},{3,5},{4,2},{5,3},{6,0},{7,1},{8,14},{9,15},{10,... | collective-permute-start | bytes 98312 | tf_op jit(solution)/shard_map/ppermute | solution.py:18
  69.3 5.0 %collective-permute-start.15 = (bf16[128,128]{1,0:T(8,128)(2,1)}, bf16[128,128]{1,0:T(8,128)(2,1)S(1)}, u32[]{:S(2)}, u32[]{:S(2)}) collective-permute-start(bf16[128,128]{1,0:T(8,128)(2,1)} %shard_map.153.base_ref), channel_id=1, source_target_pairs={{0,4},{1,5},{2,6},{3,7},{4,0},{5,1},{6,2},{7,3},{8,12},{9,13},{10,... | collective-permute-start | bytes 98312 | tf_op jit(solution)/shard_map/ppermute | solution.py:18
  69.3 5.0 %collective-permute-start.14 = (bf16[128,128]{1,0:T(8,128)(2,1)}, bf16[128,128]{1,0:T(8,128)(2,1)S(1)}, u32[]{:S(2)}, u32[]{:S(2)}) collective-permute-start(bf16[128,128]{1,0:T(8,128)(2,1)} %shard_map.153.base_ref), channel_id=1, source_target_pairs={{0,2},{1,3},{2,0},{3,1},{4,6},{5,7},{6,4},{7,5},{8,10},{9,11},{10,... | collective-permute-start | bytes 98312 | tf_op jit(solution)/shard_map/ppermute | solution.py:18
  75.1 7.5 %copy-start.1 = (bf16[4,128,128]{2,1,0:T(8,128)(2,1)}, bf16[4,128,128]{2,1,0:T(8,128)(2,1)S(1)}, u32[]{:S(2)}) copy-start(bf16[4,128,128]{2,1,0:T(8,128)(2,1)S(1)} %pad_maximum_fusion.1.near_ref) | copy-start | bytes 393220
  75.1 7.5 %collective-permute-start.17 = (bf16[4,128,128]{2,1,0:T(8,128)(2,1)S(1)}, bf16[4,128,128]{2,1,0:T(8,128)(2,1)S(1)}, u32[]{:S(2)}, u32[]{:S(2)}) collective-permute-start(bf16[4,128,128]{2,1,0:T(8,128)(2,1)S(1)} %pad_maximum_fusion.1.near_ref), channel_id=1, source_target_pairs={{0,1},{1,0},{2,3},{3,2},{4,5},{5,4},{6,7},{7,6},{8,9},{9,8},{10,11... | collective-permute-start | bytes 393224 | tf_op jit(solution)/shard_map/ppermute | solution.py:18
  88.0 7.6 %collective-permute-start.18 = (bf16[32,2816]{1,0:T(8,128)(2,1)}, bf16[32,2816]{1,0:T(8,128)(2,1)S(1)}, u32[]{:S(2)}, u32[]{:S(2)}) collective-permute-start(bf16[32,2816]{1,0:T(8,128)(2,1)} %get-tuple-element.36), channel_id=1, source_target_pairs={{0,8},{8,0},{16,24},{24,16},{1,9},{9,1},{17,25},{25,17},{2,10},{10... | collective-permute-start | bytes 540680 | tf_op jit(solution)/shard_map/ppermute | solution.py:18
  89.0 10.7 %collective-permute-start.19 = (bf16[32,2816]{1,0:T(8,128)(2,1)}, bf16[32,2816]{1,0:T(8,128)(2,1)S(1)}, u32[]{:S(2)}, u32[]{:S(2)}) collective-permute-start(bf16[32,2816]{1,0:T(8,128)(2,1)} %get-tuple-element.37), channel_id=1, source_target_pairs={{0,16},{8,24},{16,0},{24,8},{1,17},{9,25},{17,1},{25,9},{2,18},{10... | collective-permute-start | bytes 540680 | tf_op jit(solution)/shard_map/ppermute | solution.py:18
  90.4 9.3 %collective-permute-start.20 = (bf16[32,2816]{1,0:T(8,128)(2,1)}, bf16[32,2816]{1,0:T(8,128)(2,1)S(1)}, u32[]{:S(2)}, u32[]{:S(2)}) collective-permute-start(bf16[32,2816]{1,0:T(8,128)(2,1)} %get-tuple-element.38), channel_id=1, source_target_pairs={{0,24},{8,16},{16,8},{24,0},{1,25},{9,17},{17,9},{25,1},{2,26},{10... | collective-permute-start | bytes 540680 | tf_op jit(solution)/shard_map/ppermute | solution.py:18
  95.7 4.0 %copy-start.3 = (bf16[32,2816]{1,0:T(8,128)(2,1)}, bf16[32,2816]{1,0:T(8,128)(2,1)S(1)}, u32[]{:S(2)}) copy-start(bf16[32,2816]{1,0:T(8,128)(2,1)S(1)} %collective-permute-done.18.refs_1_) | copy-start | bytes 540676
  102.4 6.5 %collective-permute-start.23 = (bf16[32,1408]{1,0:T(8,128)(2,1)}, bf16[32,1408]{1,0:T(8,128)(2,1)S(1)}, u32[]{:S(2)}, u32[]{:S(2)}) collective-permute-start(bf16[32,1408]{1,0:T(8,128)(2,1)} %shard_map.155.refs_0_), channel_id=1, source_target_pairs={{0,24},{8,16},{16,8},{24,0},{1,25},{9,17},{17,9},{25,1},{2,26},{10... | collective-permute-start | bytes 270344 | tf_op jit(solution)/shard_map/ppermute | solution.py:18
  103.8 5.5 %collective-permute-start.22 = (bf16[32,1408]{1,0:T(8,128)(2,1)}, bf16[32,1408]{1,0:T(8,128)(2,1)S(1)}, u32[]{:S(2)}, u32[]{:S(2)}) collective-permute-start(bf16[32,1408]{1,0:T(8,128)(2,1)} %shard_map.155.refs_0_), channel_id=1, source_target_pairs={{0,16},{8,24},{16,0},{24,8},{1,17},{9,25},{17,1},{25,9},{2,18},{10... | collective-permute-start | bytes 270344 | tf_op jit(solution)/shard_map/ppermute | solution.py:18
  105.0 4.8 %collective-permute-start.21 = (bf16[32,1408]{1,0:T(8,128)(2,1)}, bf16[32,1408]{1,0:T(8,128)(2,1)S(1)}, u32[]{:S(2)}, u32[]{:S(2)}) collective-permute-start(bf16[32,1408]{1,0:T(8,128)(2,1)} %shard_map.155.refs_0_), channel_id=1, source_target_pairs={{0,8},{8,0},{16,24},{24,16},{1,9},{9,1},{17,25},{25,17},{2,10},{10... | collective-permute-start | bytes 270344 | tf_op jit(solution)/shard_map/ppermute | solution.py:18
  114.0 1.6 %collective-permute-start.24 = (bf16[4,128,128]{2,1,0:T(8,128)(2,1)}, bf16[4,128,128]{2,1,0:T(8,128)(2,1)S(1)}, u32[]{:S(2)}, u32[]{:S(2)}) collective-permute-start(bf16[4,128,128]{2,1,0:T(8,128)(2,1)} %get-tuple-element.40), channel_id=1, source_target_pairs={{0,1},{1,0},{2,3},{3,2},{4,5},{5,4},{6,7},{7,6},{8,9},{9,8},{10,11... | collective-permute-start | bytes 393224 | tf_op jit(solution)/shard_map/ppermute | solution.py:18
  117.8 4.5 %collective-permute-start.25 = (bf16[128,128]{1,0:T(8,128)(2,1)}, bf16[128,128]{1,0:T(8,128)(2,1)S(1)}, u32[]{:S(2)}, u32[]{:S(2)}) collective-permute-start(bf16[128,128]{1,0:T(8,128)(2,1)} %get-tuple-element.42), channel_id=1, source_target_pairs={{0,2},{1,3},{2,0},{3,1},{4,6},{5,7},{6,4},{7,5},{8,10},{9,11},{10,... | collective-permute-start | bytes 98312 | tf_op jit(solution)/shard_map/ppermute | solution.py:18
  117.8 5.0 %collective-permute-start.26 = (bf16[128,128]{1,0:T(8,128)(2,1)}, bf16[128,128]{1,0:T(8,128)(2,1)S(1)}, u32[]{:S(2)}, u32[]{:S(2)}) collective-permute-start(bf16[128,128]{1,0:T(8,128)(2,1)} %get-tuple-element.43), channel_id=1, source_target_pairs={{0,4},{1,5},{2,6},{3,7},{4,0},{5,1},{6,2},{7,3},{8,12},{9,13},{10,... | collective-permute-start | bytes 98312 | tf_op jit(solution)/shard_map/ppermute | solution.py:18
  119.9 5.9 %collective-permute-start.27 = (bf16[128,128]{1,0:T(8,128)(2,1)}, bf16[128,128]{1,0:T(8,128)(2,1)S(1)}, u32[]{:S(2)}, u32[]{:S(2)}) collective-permute-start(bf16[128,128]{1,0:T(8,128)(2,1)} %get-tuple-element.44), channel_id=1, source_target_pairs={{0,6},{1,7},{2,4},{3,5},{4,2},{5,3},{6,0},{7,1},{8,14},{9,15},{10,... | collective-permute-start | bytes 98312 | tf_op jit(solution)/shard_map/ppermute | solution.py:18
  (21 other events, 24.2 us)

commit v2 on v1

--- a/solution.py
+++ b/solution.py
@@ -18,8 +18,16 @@
     return lax.ppermute(value, axis, [(i, i ^ mask) for i in range(size)])
 
 
-def call(kernel, out_shape, scratch=(), **kwargs):
-    return pl.pallas_call(kernel, out_shape=out_shape, scratch_shapes=list(scratch), **kwargs)
+def call(kernel, outs, scratch=(), megabytes=8, space=pltpu.VMEM):
+    inner = pl.pallas_call(
+        kernel,
+        out_shape=[space(shape, dtype) for shape, dtype in outs],
+        scratch_shapes=list(scratch),
+        compiler_params=pltpu.CompilerParams(vmem_limit_bytes=megabytes << 20),
+    )
+    return lambda *args: inner(
+        *(pltpu.with_memory_space_constraint(arg, pltpu.VMEM) for arg in args)
+    )
 
 
 def tail_pieces(total, first_lane):
@@ -33,8 +41,33 @@
     )
 
 
-def product(left, right):
-    return jnp.dot(left, right, preferred_element_type=F32)
+def load_kernel(*refs):
+    count = len(refs) // 2
+    copies = [
+        pltpu.make_async_copy(refs[i], refs[count + i], refs[-1].at[i]) for i in range(count)
+    ]
+    for copy in copies:
+        copy.start()
+    for copy in copies:
+        copy.wait()
+
+
+def load(*arrays):
+    size = sum(a.size * a.dtype.itemsize for a in arrays)
+    return pl.pallas_call(
+        load_kernel,
+        in_specs=[pl.BlockSpec(memory_space=pltpu.HBM)] * len(arrays),
+        out_specs=[pl.BlockSpec(memory_space=pltpu.VMEM)] * len(arrays),
+        out_shape=[pltpu.VMEM(a.shape, a.dtype) for a in arrays],
+        scratch_shapes=[pltpu.SemaphoreType.DMA((len(arrays),))],
+        cost_estimate=pl.CostEstimate(flops=16 * size, bytes_accessed=2 * size, transcendentals=0),
+        compiler_params=pltpu.CompilerParams(vmem_limit_bytes=1 << 20),
+    )(*(pltpu.with_memory_space_constraint(a, pltpu.HBM) for a in arrays))
+
+
+def product(left, right, right_dim=0):
+    dims = (((1,), (right_dim,)), ((), ()))
+    return lax.dot_general(left, right, dims, preferred_element_type=F32)
 
 
 def gather_scaled(near_ref, far_ref, gain_ref, blocks_ref, count):
@@ -56,7 +89,7 @@
         ref[...] = parts_ref[own ^ mask].astype(BF16)
 
 
-def project_kernel(near_ref, far_ref, gain_ref, *refs, count, n_weights, offsets, tail, local):
+def project_kernel(near_ref, far_ref, gain_ref, *refs, count, n_weights, offsets, tail, local, dim):
     weights, outs = refs[:n_weights], refs[n_weights:-2]
     blocks_ref, parts_ref = refs[-2:]
     rows, squares = gather_scaled(near_ref, far_ref, gain_ref, blocks_ref, count)
@@ -72,11 +105,11 @@
     put(zero, parts_ref.shape[2] - LANES)
     put(pieces, start)
     for weight, at in zip(weights, offsets):
-        put(product(rows, weight[...]), at)
+        put(product(rows, weight[...], dim), at)
     spread(parts_ref, outs[0], outs[1:])
 
 
-def project(near, far, gain, weights, offsets, tail, width, n_kv):
+def project(near, far, gains, weights, offsets, tail, width, n_kv, dim=0):
     count, seqs, block = near.shape
     local = seqs // n_kv
     kernel = functools.partial(
@@ -86,77 +119,122 @@
         offsets=offsets,
         tail=tail,
         local=local,
-    )
-    outs = [jax.ShapeDtypeStruct((local, width), F32)]
-    outs += [jax.ShapeDtypeStruct((local, width), BF16)] * (n_kv - 1)
+        dim=dim,
+    )
+    outs = [((local, width), F32)] + [((local, width), BF16)] * (n_kv - 1)
     scratch = [
         pltpu.VMEM((PAIR * count, seqs, block), BF16),
         pltpu.VMEM((n_kv, local, width), F32),
     ]
-    gains = gain.reshape(PAIR * count, 1, block)
     return call(kernel, outs, scratch)(near, far, gains, *weights)
 
 
-def recur_kernel(*refs, n_parts, model, heads, keys, values):
-    parts = refs[:n_parts]
-    bound_ref, gain_ref, state_ref, new_ref, normed_ref = refs[n_parts:]
-    raw = parts[0][...]
+def halves(value):
+    high = value.astype(BF16).astype(F32)
+    return high, value - high
+
+
+def diagonal(tile):
+    row = lax.broadcasted_iota(jnp.int32, tile.shape, 0)
+    return jnp.concatenate([jnp.where(row == s, tile, 0.0) for s in range(tile.shape[0])], axis=1)
+
+
+def outer(left, right):
+    left, right = jnp.concatenate(left, axis=0), jnp.concatenate(right, axis=0)
+    dims = (((0,), (0,)), ((), ()))
+    return lax.dot_general(left.astype(BF16), right.astype(BF16), dims, preferred_element_type=F32)
+
+
+def gates(parts, bound_ref, model, hid, vid, span=slice(None)):
+    raw = parts[0][span, :]
     for ref in parts[1:]:
-        raw = raw + ref[...].astype(F32)
+        raw = raw + ref[span, :].astype(F32)
     total = jnp.sum(raw[:, -LANES:], axis=1, keepdims=True)
     raw = raw * lax.rsqrt(total / model + EPS)
-    local = raw.shape[0]
-    hid = heads * keys
     bound = bound_ref[...]
-    query = jax.nn.silu(raw[:, :hid])
     forget_raw = raw[:, hid : 2 * hid]
     forget = bound + (1.0 - bound) * jax.nn.sigmoid(forget_raw)
     keyvec = (1.0 - bound) * jax.nn.sigmoid(-forget_raw)
-    value = raw[:, 2 * hid : 2 * hid + heads * values]
-    out_gate = jax.nn.silu(raw[:, 2 * hid + heads * values : 2 * (hid + heads * values)])
+    return raw, forget, keyvec, raw[:, 2 * hid : 2 * hid + vid]
+
+
+def read_kernel(*refs, n_parts, model, step):
+    parts = refs[:n_parts]
+    bound_ref, gain_ref, state_ref, normed_ref = refs[n_parts:]
+    local, heads, keys, values = state_ref.shape
+    hid, vid = heads * keys, heads * values
+    row = lax.broadcasted_iota(jnp.int32, (step, values), 0)
+    raw, forget, keyvec, value = gates(parts, bound_ref, model, hid, vid)
+    query = jax.nn.silu(raw[:, :hid])
+    out_gate = jax.nn.silu(raw[:, 2 * hid + vid : 2 * (hid + vid)])
+    for at in range(0, local, step):
+        for h in range(heads):
+            rows = slice(at, at + step)
+            lanes = slice(h * keys, (h + 1) * keys)
+            to = slice(h * values, (h + 1) * values)
+            q, f, k = (v[rows, lanes] for v in (query, forget, keyvec))
+            v = value[rows, to]
+            old = jnp.concatenate([state_ref[s, h] for s in range(at, at + step)], axis=1)
+            old = jnp.concatenate([piece.astype(BF16) for piece in halves(old)], axis=0)
+            left = jnp.concatenate(halves(q * f), axis=0).astype(BF16)
+            read = product(jnp.concatenate([left, left], axis=1), old)
+            read = read[:step] + read[step:]
+            head_out = jnp.sum(q * k, axis=1, keepdims=True) * v
+            for s in range(step):
+                head_out += jnp.where(row == s, read[:, s * values : (s + 1) * values], 0.0)
+            scale = lax.rsqrt(jnp.mean(head_out * head_out, axis=1, keepdims=True) + EPS)
+            normed = head_out * scale * gain_ref[...] * out_gate[rows, to]
+            normed_ref[rows, to] = normed.astype(BF16)
+
+
+def update_kernel(*refs, n_parts, model, step):
+    parts = refs[:n_parts]
+    bound_ref, state_ref, _, new_ref, token_ref = refs[n_parts:]
+    token_ref[...] = jnp.zeros(token_ref.shape, F32)
+    _, heads, keys, values = state_ref.shape
+    hid, vid = heads * keys, heads * values
+    start = pl.multiple_of(pl.program_id(0) * step, step)
+    _, forget, keyvec, value = gates(parts, bound_ref, model, hid, vid, pl.ds(start, step))
+    ones = diagonal(jnp.ones((step, values), F32))
     for h in range(heads):
-        span = slice(h * keys, (h + 1) * keys)
-        columns = jnp.concatenate([query[:, span], forget[:, span], keyvec[:, span]], axis=0).T
-        spread_values = slice(h * values, (h + 1) * values)
-        rows = []
-        for s in range(local):
-            q = columns[:, s : s + 1]
-            f = columns[:, local + s : local + s + 1]
-            k = columns[:, 2 * local + s : 2 * local + s + 1]
-            new = f * state_ref[s, h] + k * value[s : s + 1, spread_values]
-            new_ref[s, h] = new
-            rows.append(jnp.sum(q * new, axis=0, keepdims=True))
-        head_out = jnp.concatenate(rows, axis=0)
-        scale = lax.rsqrt(jnp.mean(head_out * head_out, axis=1, keepdims=True) + EPS)
-        normed = head_out * scale * gain_ref[...] * out_gate[:, spread_values]
-        normed_ref[:, spread_values] = normed.astype(BF16)
-
-
-def recur(parts, lower_bound, head_gain, state, model):
+        lanes = slice(h * keys, (h + 1) * keys)
+        to = slice(h * values, (h + 1) * values)
+        decay = outer(halves(forget[:, lanes]), (ones, ones))
+        k_high, k_low = halves(keyvec[:, lanes])
+        v_high, v_low = (diagonal(piece) for piece in halves(value[:, to]))
+        added = outer((k_high, k_high, k_low, k_low), (v_high, v_low, v_high, v_low))
+        for s in range(step):
+            cols = slice(s * values, (s + 1) * values)
+            new_ref[s, h] = decay[:, cols] * state_ref[start + s, h] + added[:, cols]
+
+
+def read_state(parts, bound, head_gain, state, model):
+    local, heads, _, values = state.shape
+    kernel = functools.partial(read_kernel, n_parts=len(parts), model=model, step=8)
+    outs = [((local, heads * values), BF16)]
+    return call(kernel, outs, megabytes=12)(*parts, bound, head_gain.reshape(1, values), state)[0]
+
+
+def update_state(parts, bound, state, model, after):
     local, heads, keys, values = state.shape
     step = 8
-    width = parts[0].shape[1]
-    kernel = functools.partial(
-        recur_kernel, n_parts=len(parts), model=model, heads=heads, keys=keys, values=values
-    )
-    row = lambda i: (i, 0)
-    fixed = lambda i: (0, 0)
-    cube = pl.BlockSpec((step, heads, keys, values), lambda i: (i, 0, 0, 0))
+    kernel = functools.partial(update_kernel, n_parts=len(parts), model=model, step=step)
+    whole = pl.BlockSpec(memory_space=pltpu.VMEM)
+    args = *parts, bound, state, after
     return pl.pallas_call(
         kernel,
         grid=(local // step,),
-        in_specs=[pl.BlockSpec((step, width), row)] * len(parts)
-        + [
-            pl.BlockSpec((1, heads * keys), fixed),
-            pl.BlockSpec((1, values), fixed),
-            cube,
+        in_specs=[whole] * len(args),
+        out_specs=[
+            pl.BlockSpec((step, heads, keys, values), lambda i: (i, 0, 0, 0)),
+            whole,
         ],
-        out_specs=[cube, pl.BlockSpec((step, heads * values), row)],
-        out_shape=[
-            jax.ShapeDtypeStruct(state.shape, F32),
-            jax.ShapeDtypeStruct((local, heads * values), BF16),
-        ],
-    )(*parts, lower_bound.reshape(1, heads * keys), head_gain.reshape(1, values), state)
+        out_shape=[jax.ShapeDtypeStruct(state.shape, F32), pltpu.VMEM((8, LANES), F32)],
+        cost_estimate=pl.CostEstimate(
+            flops=64 * state.size, bytes_accessed=8 * state.size, transcendentals=0
+        ),
+        compiler_params=pltpu.CompilerParams(vmem_limit_bytes=12 << 20),
+    )(*(pltpu.with_memory_space_constraint(v, pltpu.VMEM) for v in args))
 
 
 def mix_kernel(*refs, n_parts, local, count):
@@ -183,10 +261,7 @@
     seqs = local * n_kv
     block = weight.shape[1] // (PAIR * count)
     kernel = functools.partial(mix_kernel, n_parts=n_kv, local=local, count=count)
-    outs = [
-        jax.ShapeDtypeStruct((count, seqs, block), F32),
-        jax.ShapeDtypeStruct((count, seqs, block), BF16),
-    ]
+    outs = [((count, seqs, block), F32), ((count, seqs, block), BF16)]
     scratch = [
         pltpu.VMEM((n_kv, local, width), BF16),
         pltpu.VMEM((PAIR * count, seqs, block), F32),
@@ -211,16 +286,51 @@
 def reduce_tp(keep, send, base, n_tp):
     count, seqs, block = keep.shape
     far = exchange(send, "tp", n_tp, 1)
-    outs = [jax.ShapeDtypeStruct((seqs, block), F32)]
-    outs += [jax.ShapeDtypeStruct((seqs, block), BF16)] * (count - 1)
+    outs = [((seqs, block), F32)] + [((seqs, block), BF16)] * (count - 1)
     own, *sends = call(fold_kernel, outs)(keep, far)
     got = [exchange(v, "tp", n_tp, PAIR * k) for k, v in enumerate(sends, 1)]
-    return call(finish_kernel, jax.ShapeDtypeStruct((seqs, block), BF16))(base, own, *got)
-
-
-def gather_tp(block, n_tp):
+    finish = call(finish_kernel, [((seqs, block), BF16)], space=jax.ShapeDtypeStruct)
+    return finish(base, own, *got)[0]
+
+
+def narrow_kernel(keep_ref, far_ref, own_ref, send_ref):
+    for z in range(keep_ref.shape[0]):
+        total = keep_ref[z] + far_ref[z].astype(F32)
+        own_ref[z] = total
+        send_ref[z] = total.astype(BF16)
+
+
+def settle_kernel(near_ref, own_ref, *refs):
+    count = own_ref.shape[0]
+    z = lax.axis_index("tp") // PAIR
+    for k in range(count):
+        total = near_ref[k].astype(F32) + own_ref[z ^ k]
+        for ref in refs[:-2]:
+            total = total + ref[z ^ k].astype(F32)
+        refs[-1][k] = total.astype(BF16)
+
+
+def sum_tp(keep, send, near, update, n_tp):
+    count, seqs, block = keep.shape
+    far = exchange(send, "tp", n_tp, 1)
+    shape = (count, seqs, block)
+    own, narrow = call(narrow_kernel, [(shape, F32), (shape, BF16)])(keep, far)
+    got = [exchange(narrow, "tp", n_tp, PAIR * k) for k in range(1, count)]
+    updated, token = update(own)
+    mine = call(settle_kernel, [(shape, BF16)])(near, own, *got, token)[0]
+    return mine, exchange(mine, "tp", n_tp, 1), updated
+
+
+def stack_kernel(*refs, count):
+    for k in range(count):
+        refs[-1][k] = refs[k][...]
+
+
+def gather_tp(block, held, n_tp):
     count = n_tp // PAIR
-    near = jnp.stack([block] + [exchange(block, "tp", n_tp, PAIR * k) for k in range(1, count)])
+    blocks = [held] + [exchange(block, "tp", n_tp, PAIR * k) for k in range(1, count)]
+    kernel = functools.partial(stack_kernel, count=count)
+    near = call(kernel, [((count, *block.shape), BF16)])(*blocks)[0]
     return near, exchange(near, "tp", n_tp, 1)
 
 
@@ -261,31 +371,33 @@
     local = state.shape[0]
     kv_masks = range(1, n_kv)
 
-    near, far = gather_tp(residual, n_tp)
-    weights = (w_query, w_forget, w_input, w_outgate)
+    gains = mixer_gain.reshape(n_tp, 1, -1)
+    gains, held, *weights = load(gains, residual, w_query, w_forget, w_input, w_outgate)
+    near, far = gather_tp(residual, held, n_tp)
     offsets, at = [], 0
     for weight in weights:
         offsets.append(at)
         at += weight.shape[1]
-    own, *sends = project(near, far, mixer_gain, weights, offsets, at, at + LANES, n_kv)
+    own, *sends = project(near, far, gains, weights, offsets, at, at + LANES, n_kv)
+    (held,) = load(state)
     parts = [own] + [exchange(v, "kv", n_kv, m) for m, v in zip(kv_masks, sends)]
-    new_state, normed = recur(parts, lower_bound, head_gain, state, model)
-
-    parts = [normed] + [exchange(normed, "kv", n_kv, m) for m in kv_masks]
-    keep, send = mix(parts, w_mix_out, count)
-    after_mix = reduce_tp(keep, send, residual, n_tp)
-
-    near, far = gather_tp(after_mix, n_tp)
+    bound = lower_bound.reshape(1, -1)
+    normed = read_state(parts, bound, head_gain, held, model)
+
+    rows = [normed] + [exchange(normed, "kv", n_kv, m) for m in kv_masks]
+    keep, send = mix(rows, w_mix_out, count)
+    update = functools.partial(update_state, parts, bound, held, model)
+    near, far, new_state = sum_tp(keep, send, near, update, n_tp)
+    after_mix = near[0]
+
     units = w_gate.shape[1]
     padded = (units + 3 + LANES - 1) // LANES * LANES
     own, *sends = project(
-        near, far, ffn_gain, (w_gate, w_up), (0, padded), units, 2 * padded, n_kv
+        near, far, ffn_gain.reshape(n_tp, 1, -1), (w_gate.T, w_up.T), (0, padded), units, 2 * padded, n_kv, 1
     )
     parts = [own] + [exchange(v, "kv", n_kv, m) for m, v in zip(kv_masks, sends)]
-    hidden = call(
-        functools.partial(hidden_kernel, model=model, tail=units),
-        jax.ShapeDtypeStruct((local, padded), BF16),
-    )(*parts)
+    kernel = functools.partial(hidden_kernel, model=model, tail=units)
+    hidden = call(kernel, [((local, padded), BF16)])(*parts)[0]
     parts = [hidden] + [exchange(hidden, "kv", n_kv, m) for m in kv_masks]
     keep, send = mix(parts, w_down, count)
     return reduce_tp(keep, send, after_mix, n_tp), new_state

time: 128 us -> 80.3 us (0.63)
  Pallas kernels: 36.1 us -> 17.2 us
  local copies, waits for them, and re-layouts: 14.1 us -> 0.04 us
  waiting for transfers between devices: 42.4 us -> 33 us
  starting transfers between devices: 33 us -> 29.1 us
  other arithmetic: 1.55 us -> 0 us
    pallas_call x10 -> x14, Pallas kernels: 36.1 us -> 17.2 us  [the longest x11 6.36 us: call(): inner(*(pltpu.with_memory_space_constraint(arg, pltpu.VMEM) for arg in ar...]
    unnamed x52 -> x14, local copies, waits for them, and re-layouts: 14.1 us -> 0.04 us
    ppermute x28 -> x25, waiting for transfers between devices: 42.4 us -> 33 us  [exchange(): return lax.ppermute(value, axis, [(i, i ^ mask) for i in range(size)])]
    ppermute x28 -> x25, starting transfers between devices: 33 us -> 29.1 us  [exchange(): return lax.ppermute(value, axis, [(i, i ^ mask) for i in range(size)])]
    another operation x2 -> x0, other arithmetic: 1.55 us -> none  [gather_tp(): jnp.stack([block] + [exchange(block, 'tp', n_tp, PAIR * k) for k in range...]
  transfers between devices with their start and end apart: 28 -> 25, of which waited for: 24 -> 18; matrix products, arithmetic and copies ran while one was open for 6% -> 0% of each run, Pallas kernels for 0% -> 14%
where the time goes in v2:
time: 80.3 us; the launch traced here: 80.1 us
  waiting for transfers between devices  33 us (41%)
  starting transfers between devices  29.1 us (36%)
  Pallas kernels  17.2 us (21%)
  between operations  0.81 us (1%)
    ppermute x25, waiting for transfers between devices, exchange(): return lax.ppermute(value, axis, [(i, i ^ mask) for i in range(size)])  33 us
    ppermute x25, starting transfers between devices, exchange(): return lax.ppermute(value, axis, [(i, i ^ mask) for i in range(size)])  29.1 us
    pallas_call x11, Pallas kernels, call(): inner(*(pltpu.with_memory_space_constraint(arg, pltpu.VMEM) for arg in ar...  6.36 us
    pallas_call x2, Pallas kernels, load(): pl.pallas_call(load_kernel, in_specs=[pl.BlockSpec(memory_space=pltpu.HBM...  5.65 us
    pallas_call x1, Pallas kernels, update_state(): pl.pallas_call(kernel, grid=(local // step,), in_specs=[whole] * len(args...  5.18 us
  transfers between devices with their start and end apart: 25, of which 18 were waited for; matrix products, arithmetic and copies ran while one was open for 0% of the time, Pallas kernels for 14%

profile of v2, /device:TPU:0, one launch (start us, length us, event | category | flops | bytes accessed | tf_op | source)
XLA Modules:
  0.0 80.1 jit_solution(4196884488037517741)
XLA Ops:
  0.6 3.1 %collective-permute-start = (bf16[128,128]{1,0:T(8,128)(2,1)}, bf16[128,128]{1,0:T(8,128)(2,1)S(1)}, u32[]{:S(2)}, u32[]{:S(2)}) collective-permute-start(bf16[128,128]{1,0:T(8,128)(2,1)} %refs_1_.1), channel_id=1, source_target_pairs={{0,2},{1,3},{2,0},{3,1},{4,6},{5,7},{6,4},{7,5},{8,10},{9,11},{10,... | collective-permute-start | bytes 98312 | tf_op jit(solution)/shard_map/ppermute | solution.py:18
  3.7 2.5 %collective-permute-start.2 = (bf16[128,128]{1,0:T(8,128)(2,1)}, bf16[128,128]{1,0:T(8,128)(2,1)S(1)}, u32[]{:S(2)}, u32[]{:S(2)}) collective-permute-start(bf16[128,128]{1,0:T(8,128)(2,1)} %refs_1_.1), channel_id=1, source_target_pairs={{0,6},{1,7},{2,4},{3,5},{4,2},{5,3},{6,0},{7,1},{8,14},{9,15},{10,... | collective-permute-start | bytes 98312 | tf_op jit(solution)/shard_map/ppermute | solution.py:18
  6.3 2.3 %shard_map.149 = (f32[8,1,128]{2,1,0:T(1,128)S(1)}, bf16[128,128]{1,0:T(8,128)(2,1)S(1)}, bf16[1024,512]{1,0:T(8,128)(2,1)S(1)}, bf16[1024,512]{1,0:T(8,128)(2,1...) custom-call(f32[8,1,128]{2,1,0:T(1,128)} %bitcast.14, bf16[128,128]{1,0:T(8,128)(2,1)} %refs_1_.1, ...), custom_call_target="tpu_custom_call" | custom-call | flops 67698688 | bytes 8462336 | tf_op jit(solution)/shard_map/pallas_call | solution.py:57
  8.6 1.5 %collective-permute-done.2.refs_3_ = bf16[128,128]{1,0:T(8,128)(2,1)S(1)} collective-permute-done((bf16[128,128]{1,0:T(8,128)(2,1)}, bf16[128,128]{1,0:T(8,128)(2,1)S(1)}, u32[]{:S(2)}, u32[]{:S(2)}) %collective-permute-start.2) | collective-permute-done | bytes 32800 | tf_op jit(solution)/shard_map/ppermute | solution.py:18
  10.1 1.5 %collective-permute-done.1.refs_2_ = bf16[128,128]{1,0:T(8,128)(2,1)S(1)} collective-permute-done((bf16[128,128]{1,0:T(8,128)(2,1)}, bf16[128,128]{1,0:T(8,128)(2,1)S(1)}, u32[]{:S(2)}, u32[]{:S(2)}) %collective-permute-start.1) | collective-permute-done | bytes 32800 | tf_op jit(solution)/shard_map/ppermute | solution.py:18
  11.7 1.3 %collective-permute-done.3.far_ref = bf16[4,128,128]{2,1,0:T(8,128)(2,1)S(1)} collective-permute-done((bf16[4,128,128]{2,1,0:T(8,128)(2,1)S(1)}, bf16[4,128,128]{2,1,0:T(8,128)(2,1)S(1)}, u32[]{:S(2)}, u32[]{:S(2)}) %collective-permute-start.3) | collective-permute-done | bytes 131104 | tf_op jit(solution)/shard_map/ppermute | solution.py:18
  13.8 1.6 %collective-permute-start.4 = (bf16[32,2176]{1,0:T(8,128)(2,1)S(1)}, bf16[32,2176]{1,0:T(8,128)(2,1)S(1)}, u32[]{:S(2)}, u32[]{:S(2)}) collective-permute-start(bf16[32,2176]{1,0:T(8,128)(2,1)S(1)} %get-tuple-element.35), channel_id=1, source_target_pairs={{0,8},{8,0},{16,24},{24,16},{1,9},{9,1},{17,25},{25,17},{2,10},{10... | collective-permute-start | bytes 417800 | tf_op jit(solution)/shard_map/ppermute | solution.py:18
  15.4 1.5 %collective-permute-start.5 = (bf16[32,2176]{1,0:T(8,128)(2,1)S(1)}, bf16[32,2176]{1,0:T(8,128)(2,1)S(1)}, u32[]{:S(2)}, u32[]{:S(2)}) collective-permute-start(bf16[32,2176]{1,0:T(8,128)(2,1)S(1)} %get-tuple-element.36), channel_id=1, source_target_pairs={{0,16},{8,24},{16,0},{24,8},{1,17},{9,25},{17,1},{25,9},{2,18},{10... | collective-permute-start | bytes 417800 | tf_op jit(solution)/shard_map/ppermute | solution.py:18
  17.4 3.4 %shard_map.152.refs_6_.refs_5_ = f32[32,4,128,128]{3,2,1,0:T(8,128)S(1)} custom-call(f32[32,4,128,128]{3,2,1,0:T(8,128)} %refs_0_.1), custom_call_target="tpu_custom_call" | custom-call | flops 134217728 | bytes 16777216 | tf_op jit(solution)/shard_map/pallas_call | solution.py:57
  20.8 3.0 %collective-permute-done.5.refs_2_ = bf16[32,2176]{1,0:T(8,128)(2,1)S(1)} collective-permute-done((bf16[32,2176]{1,0:T(8,128)(2,1)S(1)}, bf16[32,2176]{1,0:T(8,128)(2,1)S(1)}, u32[]{:S(2)}, u32[]{:S(2)}) %collective-permute-start.5) | collective-permute-done | bytes 139296 | tf_op jit(solution)/shard_map/ppermute | solution.py:18
  23.9 1.5 %shard_map.153.refs_0_ = bf16[32,512]{1,0:T(8,128)(2,1)S(1)} custom-call(f32[32,2176]{1,0:T(8,128)S(1)} %get-tuple-element.34.refs_0_, bf16[32,2176]{1,0:T(8,128)(2,1)S(1)} %collective-permute-done.4.refs_1_, bf16[32,2176]{1,0:T(8,128)(2,1)S(1)} %collective-permute-done.5.refs_2_, bf16[32,2176]{1,0:T(8,128)(2,1)S(1)} %collective-permute-done.6.refs_3_, ...), custom_call_target="tpu_custom_call" | custom-call | tf_op jit(solution)/shard_map/pallas_call | solution.py:28
  25.4 1.5 %collective-permute-start.9 = (bf16[32,512]{1,0:T(8,128)(2,1)S(1)}, bf16[32,512]{1,0:T(8,128)(2,1)S(1)}, u32[]{:S(2)}, u32[]{:S(2)}) collective-permute-start(bf16[32,512]{1,0:T(8,128)(2,1)S(1)} %shard_map.153.refs_0_), channel_id=1, source_target_pairs={{0,24},{8,16},{16,8},{24,0},{1,25},{9,17},{17,9},{25,1},{2,26},{10... | collective-permute-start | bytes 98312 | tf_op jit(solution)/shard_map/ppermute | solution.py:18
  26.9 1.2 %collective-permute-start.8 = (bf16[32,512]{1,0:T(8,128)(2,1)S(1)}, bf16[32,512]{1,0:T(8,128)(2,1)S(1)}, u32[]{:S(2)}, u32[]{:S(2)}) collective-permute-start(bf16[32,512]{1,0:T(8,128)(2,1)S(1)} %shard_map.153.refs_0_), channel_id=1, source_target_pairs={{0,16},{8,24},{16,0},{24,8},{1,17},{9,25},{17,1},{25,9},{2,18},{10... | collective-permute-start | bytes 98312 | tf_op jit(solution)/shard_map/ppermute | solution.py:18
  28.9 1.3 %collective-permute-done.9.refs_3_ = bf16[32,512]{1,0:T(8,128)(2,1)S(1)} collective-permute-done((bf16[32,512]{1,0:T(8,128)(2,1)S(1)}, bf16[32,512]{1,0:T(8,128)(2,1)S(1)}, u32[]{:S(2)}, u32[]{:S(2)}) %collective-permute-start.9) | collective-permute-done | bytes 32800 | tf_op jit(solution)/shard_map/ppermute | solution.py:18
  30.8 1.2 %collective-permute-done.7.refs_1_ = bf16[32,512]{1,0:T(8,128)(2,1)S(1)} collective-permute-done((bf16[32,512]{1,0:T(8,128)(2,1)S(1)}, bf16[32,512]{1,0:T(8,128)(2,1)S(1)}, u32[]{:S(2)}, u32[]{:S(2)}) %collective-permute-start.7) | collective-permute-done | bytes 32800 | tf_op jit(solution)/shard_map/ppermute | solution.py:18
  32.5 1.3 %collective-permute-done.10.far_ref = bf16[4,128,128]{2,1,0:T(8,128)(2,1)S(1)} collective-permute-done((bf16[4,128,128]{2,1,0:T(8,128)(2,1)S(1)}, bf16[4,128,128]{2,1,0:T(8,128)(2,1)S(1)}, u32[]{:S(2)}, u32[]{:S(2)}) %collective-permute-start.10) | collective-permute-done | bytes 131104 | tf_op jit(solution)/shard_map/ppermute | solution.py:18
  33.8 1.3 %collective-permute-start.13 = (bf16[4,128,128]{2,1,0:T(8,128)(2,1)S(1)}, bf16[4,128,128]{2,1,0:T(8,128)(2,1)S(1)}, u32[]{:S(2)}, u32[]{:S(2)}) collective-permute-start(bf16[4,128,128]{2,1,0:T(8,128)(2,1)S(1)} %get-tuple-element.41), channel_id=1, source_target_pairs={{0,6},{1,7},{2,4},{3,5},{4,2},{5,3},{6,0},{7,1},{8,14},{9,15},{10,... | collective-permute-start | bytes 393224 | tf_op jit(solution)/shard_map/ppermute | solution.py:18
  35.8 2.5 %collective-permute-start.11 = (bf16[4,128,128]{2,1,0:T(8,128)(2,1)S(1)}, bf16[4,128,128]{2,1,0:T(8,128)(2,1)S(1)}, u32[]{:S(2)}, u32[]{:S(2)}) collective-permute-start(bf16[4,128,128]{2,1,0:T(8,128)(2,1)S(1)} %get-tuple-element.41), channel_id=1, source_target_pairs={{0,2},{1,3},{2,0},{3,1},{4,6},{5,7},{6,4},{7,5},{8,10},{9,11},{10,... | collective-permute-start | bytes 393224 | tf_op jit(solution)/shard_map/ppermute | solution.py:18
  38.3 5.2 %shard_map.156 = (f32[32,4,128,128]{3,2,1,0:T(8,128)}, f32[8,128]{1,0:T(8,128)S(1)}) custom-call(f32[32,2176]{1,0:T(8,128)S(1)} %get-tuple-element.34.refs_0_, bf16[32,2176]{1,0:T(8,128)(2,1)S(1)} %collective-permute-done.4.refs_1_, bf16[32,2176]{1,0:T(8,128)(2,1)S(1)} %collective-permute-done.5.refs_2_, ...), custom_call_target="tpu_custom_call" | custom-call | flops 134217728 | bytes 16777216 | tf_op jit(solution)/shard_map/pallas_call | solution.py:224
  43.5 4.3 %collective-permute-done.12.refs_1_ = bf16[4,128,128]{2,1,0:T(8,128)(2,1)S(1)} collective-permute-done((bf16[4,128,128]{2,1,0:T(8,128)(2,1)S(1)}, bf16[4,128,128]{2,1,0:T(8,128)(2,1)S(1)}, u32[]{:S(2)}, u32[]{:S(2)}) %collective-permute-start.12) | collective-permute-done | bytes 131104 | tf_op jit(solution)/shard_map/ppermute | solution.py:18
  47.9 1.3 %collective-permute-done.14.far_ref = bf16[4,128,128]{2,1,0:T(8,128)(2,1)S(1)} collective-permute-done((bf16[4,128,128]{2,1,0:T(8,128)(2,1)S(1)}, bf16[4,128,128]{2,1,0:T(8,128)(2,1)S(1)}, u32[]{:S(2)}, u32[]{:S(2)}) %collective-permute-start.14) | collective-permute-done | bytes 131104 | tf_op jit(solution)/shard_map/ppermute | solution.py:18
  49.3 2.0 %shard_map.158 = (f32[32,2816]{1,0:T(8,128)S(1)}, bf16[32,2816]{1,0:T(8,128)(2,1)S(1)}, bf16[32,2816]{1,0:T(8,128)(2,1)S(1)}, bf16[32,2816]{1,0:T(8,128)(2,1)S(1)}) custom-call(bf16[4,128,128]{2,1,0:T(8,128)(2,1)S(1)} %shard_map.157.near_ref, bf16[4,128,128]{2,1,0:T(8,128)(2,1)S(1)} %collective-permute-done.14.far_ref, f32[8,1,128]{2,1,0:T(1,128)S(1)} %bitcast.12, ...), custom_call_target="tpu_custom_call" | custom-call | tf_op jit(solution)/shard_map/pallas_call | solution.py:28
  52.2 1.5 %collective-permute-start.16 = (bf16[32,2816]{1,0:T(8,128)(2,1)S(1)}, bf16[32,2816]{1,0:T(8,128)(2,1)S(1)}, u32[]{:S(2)}, u32[]{:S(2)}) collective-permute-start(bf16[32,2816]{1,0:T(8,128)(2,1)S(1)} %get-tuple-element.45), channel_id=1, source_target_pairs={{0,16},{8,24},{16,0},{24,8},{1,17},{9,25},{17,1},{25,9},{2,18},{10... | collective-permute-start | bytes 540680 | tf_op jit(solution)/shard_map/ppermute | solution.py:18
  54.9 3.9 %collective-permute-done.15.refs_1_ = bf16[32,2816]{1,0:T(8,128)(2,1)S(1)} collective-permute-done((bf16[32,2816]{1,0:T(8,128)(2,1)S(1)}, bf16[32,2816]{1,0:T(8,128)(2,1)S(1)}, u32[]{:S(2)}, u32[]{:S(2)}) %collective-permute-start.15) | collective-permute-done | bytes 180256 | tf_op jit(solution)/shard_map/ppermute | solution.py:18
  58.8 3.6 %collective-permute-done.16.refs_2_ = bf16[32,2816]{1,0:T(8,128)(2,1)S(1)} collective-permute-done((bf16[32,2816]{1,0:T(8,128)(2,1)S(1)}, bf16[32,2816]{1,0:T(8,128)(2,1)S(1)}, u32[]{:S(2)}, u32[]{:S(2)}) %collective-permute-start.16) | collective-permute-done | bytes 180256 | tf_op jit(solution)/shard_map/ppermute | solution.py:18
  62.5 1.6 %collective-permute-start.20 = (bf16[32,1408]{1,0:T(8,128)(2,1)S(1)}, bf16[32,1408]{1,0:T(8,128)(2,1)S(1)}, u32[]{:S(2)}, u32[]{:S(2)}) collective-permute-start(bf16[32,1408]{1,0:T(8,128)(2,1)S(1)} %shard_map.159.refs_0_), channel_id=1, source_target_pairs={{0,24},{8,16},{16,8},{24,0},{1,25},{9,17},{17,9},{25,1},{2,26},{10... | collective-permute-start | bytes 270344 | tf_op jit(solution)/shard_map/ppermute | solution.py:18
  64.1 1.2 %collective-permute-start.19 = (bf16[32,1408]{1,0:T(8,128)(2,1)S(1)}, bf16[32,1408]{1,0:T(8,128)(2,1)S(1)}, u32[]{:S(2)}, u32[]{:S(2)}) collective-permute-start(bf16[32,1408]{1,0:T(8,128)(2,1)S(1)} %shard_map.159.refs_0_), channel_id=1, source_target_pairs={{0,16},{8,24},{16,0},{24,8},{1,17},{9,25},{17,1},{25,9},{2,18},{10... | collective-permute-start | bytes 270344 | tf_op jit(solution)/shard_map/ppermute | solution.py:18
  66.1 2.5 %collective-permute-done.20.refs_3_ = bf16[32,1408]{1,0:T(8,128)(2,1)S(1)} collective-permute-done((bf16[32,1408]{1,0:T(8,128)(2,1)S(1)}, bf16[32,1408]{1,0:T(8,128)(2,1)S(1)}, u32[]{:S(2)}, u32[]{:S(2)}) %collective-permute-start.20) | collective-permute-done | bytes 90144 | tf_op jit(solution)/shard_map/ppermute | solution.py:18
  70.6 1.3 %collective-permute-done.21.far_ref = bf16[4,128,128]{2,1,0:T(8,128)(2,1)S(1)} collective-permute-done((bf16[4,128,128]{2,1,0:T(8,128)(2,1)S(1)}, bf16[4,128,128]{2,1,0:T(8,128)(2,1)S(1)}, u32[]{:S(2)}, u32[]{:S(2)}) %collective-permute-start.21) | collective-permute-done | bytes 131104 | tf_op jit(solution)/shard_map/ppermute | solution.py:18
  72.1 1.7 %collective-permute-start.23 = (bf16[128,128]{1,0:T(8,128)(2,1)S(1)}, bf16[128,128]{1,0:T(8,128)(2,1)S(1)}, u32[]{:S(2)}, u32[]{:S(2)}) collective-permute-start(bf16[128,128]{1,0:T(8,128)(2,1)S(1)} %get-tuple-element.51), channel_id=1, source_target_pairs={{0,4},{1,5},{2,6},{3,7},{4,0},{5,1},{6,2},{7,3},{8,12},{9,13},{10,... | collective-permute-start | bytes 98312 | tf_op jit(solution)/shard_map/ppermute | solution.py:18
  73.8 2.7 %collective-permute-start.24 = (bf16[128,128]{1,0:T(8,128)(2,1)S(1)}, bf16[128,128]{1,0:T(8,128)(2,1)S(1)}, u32[]{:S(2)}, u32[]{:S(2)}) collective-permute-start(bf16[128,128]{1,0:T(8,128)(2,1)S(1)} %get-tuple-element.52), channel_id=1, source_target_pairs={{0,6},{1,7},{2,4},{3,5},{4,2},{5,3},{6,0},{7,1},{8,14},{9,15},{10,... | collective-permute-start | bytes 98312 | tf_op jit(solution)/shard_map/ppermute | solution.py:18
  77.0 2.5 %collective-permute-done.24.refs_3_ = bf16[128,128]{1,0:T(8,128)(2,1)S(1)} collective-permute-done((bf16[128,128]{1,0:T(8,128)(2,1)S(1)}, bf16[128,128]{1,0:T(8,128)(2,1)S(1)}, u32[]{:S(2)}, u32[]{:S(2)}) %collective-permute-start.24) | collective-permute-done | bytes 32800 | tf_op jit(solution)/shard_map/ppermute | solution.py:18
  (47 shorter events, 10.4 us)
Async XLA Ops:
  0.6 8.0 %collective-permute-start = (bf16[128,128]{1,0:T(8,128)(2,1)}, bf16[128,128]{1,0:T(8,128)(2,1)S(1)}, u32[]{:S(2)}, u32[]{:S(2)}) collective-permute-start(bf16[128,128]{1,0:T(8,128)(2,1)} %refs_1_.1), channel_id=1, source_target_pairs={{0,2},{1,3},{2,0},{3,1},{4,6},{5,7},{6,4},{7,5},{8,10},{9,11},{10,... | collective-permute-start | bytes 98312 | tf_op jit(solution)/shard_map/ppermute | solution.py:18
  3.7 6.4 %collective-permute-start.2 = (bf16[128,128]{1,0:T(8,128)(2,1)}, bf16[128,128]{1,0:T(8,128)(2,1)S(1)}, u32[]{:S(2)}, u32[]{:S(2)}) collective-permute-start(bf16[128,128]{1,0:T(8,128)(2,1)} %refs_1_.1), channel_id=1, source_target_pairs={{0,6},{1,7},{2,4},{3,5},{4,2},{5,3},{6,0},{7,1},{8,14},{9,15},{10,... | collective-permute-start | bytes 98312 | tf_op jit(solution)/shard_map/ppermute | solution.py:18
  6.2 5.4 %collective-permute-start.1 = (bf16[128,128]{1,0:T(8,128)(2,1)}, bf16[128,128]{1,0:T(8,128)(2,1)S(1)}, u32[]{:S(2)}, u32[]{:S(2)}) collective-permute-start(bf16[128,128]{1,0:T(8,128)(2,1)} %refs_1_.1), channel_id=1, source_target_pairs={{0,4},{1,5},{2,6},{3,7},{4,0},{5,1},{6,2},{7,3},{8,12},{9,13},{10,... | collective-permute-start | bytes 98312 | tf_op jit(solution)/shard_map/ppermute | solution.py:18
  11.6 1.4 %collective-permute-start.3 = (bf16[4,128,128]{2,1,0:T(8,128)(2,1)S(1)}, bf16[4,128,128]{2,1,0:T(8,128)(2,1)S(1)}, u32[]{:S(2)}, u32[]{:S(2)}) collective-permute-start(bf16[4,128,128]{2,1,0:T(8,128)(2,1)S(1)} %shard_map.150.near_ref), channel_id=1, source_target_pairs={{0,1},{1,0},{2,3},{3,2},{4,5},{5,4},{6,7},{7,6},{8,9},{9,8},{10,11... | collective-permute-start | bytes 393224 | tf_op jit(solution)/shard_map/ppermute | solution.py:18
  13.8 7.0 %collective-permute-start.4 = (bf16[32,2176]{1,0:T(8,128)(2,1)S(1)}, bf16[32,2176]{1,0:T(8,128)(2,1)S(1)}, u32[]{:S(2)}, u32[]{:S(2)}) collective-permute-start(bf16[32,2176]{1,0:T(8,128)(2,1)S(1)} %get-tuple-element.35), channel_id=1, source_target_pairs={{0,8},{8,0},{16,24},{24,16},{1,9},{9,1},{17,25},{25,17},{2,10},{10... | collective-permute-start | bytes 417800 | tf_op jit(solution)/shard_map/ppermute | solution.py:18
  15.4 8.4 %collective-permute-start.5 = (bf16[32,2176]{1,0:T(8,128)(2,1)S(1)}, bf16[32,2176]{1,0:T(8,128)(2,1)S(1)}, u32[]{:S(2)}, u32[]{:S(2)}) collective-permute-start(bf16[32,2176]{1,0:T(8,128)(2,1)S(1)} %get-tuple-element.36), channel_id=1, source_target_pairs={{0,16},{8,24},{16,0},{24,8},{1,17},{9,25},{17,1},{25,9},{2,18},{10... | collective-permute-start | bytes 417800 | tf_op jit(solution)/shard_map/ppermute | solution.py:18
  16.9 6.9 %copy-start.4 = (f32[512]{0:T(512)S(1)}, f32[512]{0:T(512)}, u32[]{:S(2)}) copy-start(f32[512]{0:T(512)} %param.20) | copy-start | bytes 6148
  16.9 6.9 %copy-start.6 = (f32[128]{0:T(128)S(1)}, f32[128]{0:T(128)}, u32[]{:S(2)}) copy-start(f32[128]{0:T(128)} %param.22) | copy-start | bytes 1540
  16.9 6.9 %collective-permute-start.6 = (bf16[32,2176]{1,0:T(8,128)(2,1)S(1)}, bf16[32,2176]{1,0:T(8,128)(2,1)S(1)}, u32[]{:S(2)}, u32[]{:S(2)}) collective-permute-start(bf16[32,2176]{1,0:T(8,128)(2,1)S(1)} %get-tuple-element.37), channel_id=1, source_target_pairs={{0,24},{8,16},{16,8},{24,0},{1,25},{9,17},{17,9},{25,1},{2,26},{10... | collective-permute-start | bytes 417800 | tf_op jit(solution)/shard_map/ppermute | solution.py:18
  20.8 11.2 %copy-start.3 = (bf16[512,1024]{1,0:T(8,128)(2,1)S(1)}, bf16[512,1024]{1,0:T(8,128)(2,1)}, u32[]{:S(2)}) copy-start(bf16[512,1024]{1,0:T(8,128)(2,1)} %refs_4_.4) | copy-start | bytes 3145732
  23.8 25.4 %copy-start = (bf16[1024,1344]{0,1:T(8,128)(2,1)S(1)}, bf16[1024,1344]{0,1:T(8,128)(2,1)}, u32[]{:S(2)}) copy-start(bf16[1024,1344]{0,1:T(8,128)(2,1)} %param.25) | copy-start | bytes 8257540
  23.9 25.4 %copy-start.1 = (bf16[1024,1344]{0,1:T(8,128)(2,1)S(1)}, bf16[1024,1344]{0,1:T(8,128)(2,1)}, u32[]{:S(2)}) copy-start(bf16[1024,1344]{0,1:T(8,128)(2,1)} %param.26) | copy-start | bytes 8257540
  23.9 25.4 %copy-start.5 = (f32[1024]{0:T(1024)S(1)}, f32[1024]{0:T(1024)}, u32[]{:S(2)}) copy-start(f32[1024]{0:T(1024)} %param.24) | copy-start | bytes 12292
  25.4 4.8 %collective-permute-start.9 = (bf16[32,512]{1,0:T(8,128)(2,1)S(1)}, bf16[32,512]{1,0:T(8,128)(2,1)S(1)}, u32[]{:S(2)}, u32[]{:S(2)}) collective-permute-start(bf16[32,512]{1,0:T(8,128)(2,1)S(1)} %shard_map.153.refs_0_), channel_id=1, source_target_pairs={{0,24},{8,16},{16,8},{24,0},{1,25},{9,17},{17,9},{25,1},{2,26},{10... | collective-permute-start | bytes 98312 | tf_op jit(solution)/shard_map/ppermute | solution.py:18
  26.9 3.9 %collective-permute-start.8 = (bf16[32,512]{1,0:T(8,128)(2,1)S(1)}, bf16[32,512]{1,0:T(8,128)(2,1)S(1)}, u32[]{:S(2)}, u32[]{:S(2)}) collective-permute-start(bf16[32,512]{1,0:T(8,128)(2,1)S(1)} %shard_map.153.refs_0_), channel_id=1, source_target_pairs={{0,16},{8,24},{16,0},{24,8},{1,17},{9,25},{17,1},{25,9},{2,18},{10... | collective-permute-start | bytes 98312 | tf_op jit(solution)/shard_map/ppermute | solution.py:18
  28.1 3.9 %collective-permute-start.7 = (bf16[32,512]{1,0:T(8,128)(2,1)S(1)}, bf16[32,512]{1,0:T(8,128)(2,1)S(1)}, u32[]{:S(2)}, u32[]{:S(2)}) collective-permute-start(bf16[32,512]{1,0:T(8,128)(2,1)S(1)} %shard_map.153.refs_0_), channel_id=1, source_target_pairs={{0,8},{8,0},{16,24},{24,16},{1,9},{9,1},{17,25},{25,17},{2,10},{10... | collective-permute-start | bytes 98312 | tf_op jit(solution)/shard_map/ppermute | solution.py:18
  32.4 1.4 %collective-permute-start.10 = (bf16[4,128,128]{2,1,0:T(8,128)(2,1)S(1)}, bf16[4,128,128]{2,1,0:T(8,128)(2,1)S(1)}, u32[]{:S(2)}, u32[]{:S(2)}) collective-permute-start(bf16[4,128,128]{2,1,0:T(8,128)(2,1)S(1)} %get-tuple-element.39), channel_id=1, source_target_pairs={{0,1},{1,0},{2,3},{3,2},{4,5},{5,4},{6,7},{7,6},{8,9},{9,8},{10,11... | collective-permute-start | bytes 393224 | tf_op jit(solution)/shard_map/ppermute | solution.py:18
  33.8 9.6 %collective-permute-start.13 = (bf16[4,128,128]{2,1,0:T(8,128)(2,1)S(1)}, bf16[4,128,128]{2,1,0:T(8,128)(2,1)S(1)}, u32[]{:S(2)}, u32[]{:S(2)}) collective-permute-start(bf16[4,128,128]{2,1,0:T(8,128)(2,1)S(1)} %get-tuple-element.41), channel_id=1, source_target_pairs={{0,6},{1,7},{2,4},{3,5},{4,2},{5,3},{6,0},{7,1},{8,14},{9,15},{10,... | collective-permute-start | bytes 393224 | tf_op jit(solution)/shard_map/ppermute | solution.py:18
  35.1 12.6 %collective-permute-start.12 = (bf16[4,128,128]{2,1,0:T(8,128)(2,1)S(1)}, bf16[4,128,128]{2,1,0:T(8,128)(2,1)S(1)}, u32[]{:S(2)}, u32[]{:S(2)}) collective-permute-start(bf16[4,128,128]{2,1,0:T(8,128)(2,1)S(1)} %get-tuple-element.41), channel_id=1, source_target_pairs={{0,4},{1,5},{2,6},{3,7},{4,0},{5,1},{6,2},{7,3},{8,12},{9,13},{10,... | collective-permute-start | bytes 393224 | tf_op jit(solution)/shard_map/ppermute | solution.py:18
  35.8 12.0 %collective-permute-start.11 = (bf16[4,128,128]{2,1,0:T(8,128)(2,1)S(1)}, bf16[4,128,128]{2,1,0:T(8,128)(2,1)S(1)}, u32[]{:S(2)}, u32[]{:S(2)}) collective-permute-start(bf16[4,128,128]{2,1,0:T(8,128)(2,1)S(1)} %get-tuple-element.41), channel_id=1, source_target_pairs={{0,2},{1,3},{2,0},{3,1},{4,6},{5,7},{6,4},{7,5},{8,10},{9,11},{10,... | collective-permute-start | bytes 393224 | tf_op jit(solution)/shard_map/ppermute | solution.py:18
  38.3 31.6 %copy-start.2 = (bf16[1344,1024]{1,0:T(8,128)(2,1)S(1)}, bf16[1344,1024]{1,0:T(8,128)(2,1)}, u32[]{:S(2)}) copy-start(bf16[1344,1024]{1,0:T(8,128)(2,1)} %refs_4_.5) | copy-start | bytes 8257540
  47.9 1.4 %collective-permute-start.14 = (bf16[4,128,128]{2,1,0:T(8,128)(2,1)S(1)}, bf16[4,128,128]{2,1,0:T(8,128)(2,1)S(1)}, u32[]{:S(2)}, u32[]{:S(2)}) collective-permute-start(bf16[4,128,128]{2,1,0:T(8,128)(2,1)S(1)} %shard_map.157.near_ref), channel_id=1, source_target_pairs={{0,1},{1,0},{2,3},{3,2},{4,5},{5,4},{6,7},{7,6},{8,9},{9,8},{10,11... | collective-permute-start | bytes 393224 | tf_op jit(solution)/shard_map/ppermute | solution.py:18
  51.3 7.5 %collective-permute-start.15 = (bf16[32,2816]{1,0:T(8,128)(2,1)S(1)}, bf16[32,2816]{1,0:T(8,128)(2,1)S(1)}, u32[]{:S(2)}, u32[]{:S(2)}) collective-permute-start(bf16[32,2816]{1,0:T(8,128)(2,1)S(1)} %get-tuple-element.44), channel_id=1, source_target_pairs={{0,8},{8,0},{16,24},{24,16},{1,9},{9,1},{17,25},{25,17},{2,10},{10... | collective-permute-start | bytes 540680 | tf_op jit(solution)/shard_map/ppermute | solution.py:18
  52.2 10.2 %collective-permute-start.16 = (bf16[32,2816]{1,0:T(8,128)(2,1)S(1)}, bf16[32,2816]{1,0:T(8,128)(2,1)S(1)}, u32[]{:S(2)}, u32[]{:S(2)}) collective-permute-start(bf16[32,2816]{1,0:T(8,128)(2,1)S(1)} %get-tuple-element.45), channel_id=1, source_target_pairs={{0,16},{8,24},{16,0},{24,8},{1,17},{9,25},{17,1},{25,9},{2,18},{10... | collective-permute-start | bytes 540680 | tf_op jit(solution)/shard_map/ppermute | solution.py:18
  53.7 8.6 %collective-permute-start.17 = (bf16[32,2816]{1,0:T(8,128)(2,1)S(1)}, bf16[32,2816]{1,0:T(8,128)(2,1)S(1)}, u32[]{:S(2)}, u32[]{:S(2)}) collective-permute-start(bf16[32,2816]{1,0:T(8,128)(2,1)S(1)} %get-tuple-element.46), channel_id=1, source_target_pairs={{0,24},{8,16},{16,8},{24,0},{1,25},{9,17},{17,9},{25,1},{2,26},{10... | collective-permute-start | bytes 540680 | tf_op jit(solution)/shard_map/ppermute | solution.py:18
  62.5 6.1 %collective-permute-start.20 = (bf16[32,1408]{1,0:T(8,128)(2,1)S(1)}, bf16[32,1408]{1,0:T(8,128)(2,1)S(1)}, u32[]{:S(2)}, u32[]{:S(2)}) collective-permute-start(bf16[32,1408]{1,0:T(8,128)(2,1)S(1)} %shard_map.159.refs_0_), channel_id=1, source_target_pairs={{0,24},{8,16},{16,8},{24,0},{1,25},{9,17},{17,9},{25,1},{2,26},{10... | collective-permute-start | bytes 270344 | tf_op jit(solution)/shard_map/ppermute | solution.py:18
  64.1 5.2 %collective-permute-start.19 = (bf16[32,1408]{1,0:T(8,128)(2,1)S(1)}, bf16[32,1408]{1,0:T(8,128)(2,1)S(1)}, u32[]{:S(2)}, u32[]{:S(2)}) collective-permute-start(bf16[32,1408]{1,0:T(8,128)(2,1)S(1)} %shard_map.159.refs_0_), channel_id=1, source_target_pairs={{0,16},{8,24},{16,0},{24,8},{1,17},{9,25},{17,1},{25,9},{2,18},{10... | collective-permute-start | bytes 270344 | tf_op jit(solution)/shard_map/ppermute | solution.py:18
  65.3 4.5 %collective-permute-start.18 = (bf16[32,1408]{1,0:T(8,128)(2,1)S(1)}, bf16[32,1408]{1,0:T(8,128)(2,1)S(1)}, u32[]{:S(2)}, u32[]{:S(2)}) collective-permute-start(bf16[32,1408]{1,0:T(8,128)(2,1)S(1)} %shard_map.159.refs_0_), channel_id=1, source_target_pairs={{0,8},{8,0},{16,24},{24,16},{1,9},{9,1},{17,25},{25,17},{2,10},{10... | collective-permute-start | bytes 270344 | tf_op jit(solution)/shard_map/ppermute | solution.py:18
  70.6 1.4 %collective-permute-start.21 = (bf16[4,128,128]{2,1,0:T(8,128)(2,1)S(1)}, bf16[4,128,128]{2,1,0:T(8,128)(2,1)S(1)}, u32[]{:S(2)}, u32[]{:S(2)}) collective-permute-start(bf16[4,128,128]{2,1,0:T(8,128)(2,1)S(1)} %get-tuple-element.48), channel_id=1, source_target_pairs={{0,1},{1,0},{2,3},{3,2},{4,5},{5,4},{6,7},{7,6},{8,9},{9,8},{10,11... | collective-permute-start | bytes 393224 | tf_op jit(solution)/shard_map/ppermute | solution.py:18
  72.0 4.5 %collective-permute-start.22 = (bf16[128,128]{1,0:T(8,128)(2,1)S(1)}, bf16[128,128]{1,0:T(8,128)(2,1)S(1)}, u32[]{:S(2)}, u32[]{:S(2)}) collective-permute-start(bf16[128,128]{1,0:T(8,128)(2,1)S(1)} %get-tuple-element.50), channel_id=1, source_target_pairs={{0,2},{1,3},{2,0},{3,1},{4,6},{5,7},{6,4},{7,5},{8,10},{9,11},{10,... | collective-permute-start | bytes 98312 | tf_op jit(solution)/shard_map/ppermute | solution.py:18
  72.1 4.9 %collective-permute-start.23 = (bf16[128,128]{1,0:T(8,128)(2,1)S(1)}, bf16[128,128]{1,0:T(8,128)(2,1)S(1)}, u32[]{:S(2)}, u32[]{:S(2)}) collective-permute-start(bf16[128,128]{1,0:T(8,128)(2,1)S(1)} %get-tuple-element.51), channel_id=1, source_target_pairs={{0,4},{1,5},{2,6},{3,7},{4,0},{5,1},{6,2},{7,3},{8,12},{9,13},{10,... | collective-permute-start | bytes 98312 | tf_op jit(solution)/shard_map/ppermute | solution.py:18
  73.8 5.7 %collective-permute-start.24 = (bf16[128,128]{1,0:T(8,128)(2,1)S(1)}, bf16[128,128]{1,0:T(8,128)(2,1)S(1)}, u32[]{:S(2)}, u32[]{:S(2)}) collective-permute-start(bf16[128,128]{1,0:T(8,128)(2,1)S(1)} %get-tuple-element.52), channel_id=1, source_target_pairs={{0,6},{1,7},{2,4},{3,5},{4,2},{5,3},{6,0},{7,1},{8,14},{9,15},{10,... | collective-permute-start | bytes 98312 | tf_op jit(solution)/shard_map/ppermute | solution.py:18
